TPU v7x, 512 devices: a whole 4x8x8 slice. The times are simulated.
512 devices in a mesh: ep: 32 (over z, x), tp: 16 (over y, core).
Axes of the slice: x: 4, y: 8, z: 8, core: 2. Of those that a mesh axis runs over, the one named last changes fastest.
Arguments:
- mix_input: bfloat16 [12288, 2048], P('ep', 'tp'), may hold values from -6 to 6
- mix_gain: float32 [2048], replicated, may hold values from 0.1 to 1.9
- gate_b_weight: bfloat16 [2048, 2048], P(None, 'tp'), may hold values from -0.125 to 0.125
- gate_c_weight: bfloat16 [2048, 2048], P(None, 'tp'), may hold values from -0.125 to 0.125
- value_weight: bfloat16 [2048, 2048], P(None, 'tp'), may hold values from -0.125 to 0.125
- conv_weight: float32 [3, 2048], P(None, 'tp'), may hold values from -3 to 3
- out_weight: bfloat16 [2048, 2048], P('tp'), may hold values from -0.125 to 0.125
- expert_input: bfloat16 [5120, 2048], P('ep', 'tp'), may hold values from -6 to 6
- expert_gain: float32 [2048], replicated, may hold values from 0.1 to 1.9
- routes: int32 [5120, 2], P('ep'), may hold values from 0 to 31, all different within a row; in each aligned block of 160 rows (0 to 159, 160 to 319, ...) at most 20 rows name the same one
- route_weight: float32 [5120, 2], P('ep'), may hold values from 0.2 to 1
- expert_gate: bfloat16 [32, 2048, 3072], P('ep', None, 'tp'), may hold values from -0.125 to 0.125
- expert_up: bfloat16 [32, 2048, 3072], P('ep', None, 'tp'), may hold values from -0.125 to 0.125
- expert_down: bfloat16 [32, 3072, 2048], P('ep', 'tp'), may hold values from -0.109375 to 0.109375
Outputs:
- mix_output: bfloat16 [12288, 2048], P('ep', 'tp')
- expert_output: bfloat16 [5120, 2048], P('ep', 'tp')
Inputs may be any that keep to these rules, and one draw needn't show every extreme that they name: `routes`: the 2 experts of a row differ. Among the rows of one device no expert is named more than 20 times, a bound that some block reaches.
All inputs are finite; a program needn't handle non-finite values.
Results may differ from a plain program's by a relative error of at most 0.019.
Values may be sent and summed in bfloat16 or wider, within the bound.
A program may use at most 64 MiB of HBM per device.

v0:
```python
import jax
import jax.numpy as jnp
from jax import lax
from jax.sharding import PartitionSpec as P

epsilon = 1e-06
routed_scale = 2.5


def side_by_side(arrays, axis, dim, along):
    both = jnp.concatenate(arrays, axis=along)
    out, at, done = (lax.all_gather(both, axis, axis=dim, tiled=True), 0, [])
    for a in arrays:
        done.append(lax.slice_in_dim(out, at, at + a.shape[along], axis=along))
        at += a.shape[along]
    return tuple(done)


def passed_along(block, axis, distance):
    devices = range(lax.axis_size(axis))
    route = [(i - distance, i) for i in devices if i - distance in devices]
    return lax.ppermute(block, axis, route)


def project_piece(piece, gain_vector, matrices, group_count):
    widened = piece.astype(jnp.float32)
    columns = piece.shape[-1]
    scaled = (widened * gain_vector).astype(jnp.bfloat16)
    grouped = scaled.reshape(group_count, -1, columns)
    updated = tuple(
        (
            jnp.einsum("gsd,gdf->gsf", grouped, matrix, preferred_element_type=jnp.float32)
            for matrix in matrices
        )
    )
    return (updated, jnp.sum(widened * widened, axis=-1))


def local(
    mix_input,
    mix_gain,
    gate_b_weight,
    gate_c_weight,
    value_weight,
    conv_weight,
    out_weight,
    expert_input,
    expert_gain,
    routes,
    route_weight,
    expert_gate,
    expert_up,
    expert_down,
):
    ep_count = lax.axis_size("ep")
    local_experts = expert_gate.shape[0]
    model_width = mix_gain.shape[0]
    expert_count = local_experts * ep_count
    tok_local, top_count = routes.shape
    capacity = 2 * tok_local * top_count // expert_count
    feature_local = expert_input.shape[1]
    mix_rows = mix_input.shape[0]
    slot_rows = ep_count * capacity
    flat_routes = routes.reshape(-1)
    pair_count = flat_routes.shape[0]
    matches = (
        flat_routes[:, None] == lax.broadcasted_iota(jnp.int32, (pair_count, expert_count), 1)
    ).astype(jnp.int32)
    ranks = jnp.sum((jnp.cumsum(matches, axis=0) - matches) * matches, axis=1)
    slot_iota = lax.broadcasted_iota(jnp.int32, (pair_count, expert_count * capacity), 1)
    send_table = (slot_iota == (flat_routes * capacity + ranks)[:, None]).astype(jnp.bfloat16)
    back_index = (
        flat_routes % local_experts * slot_rows + flat_routes // local_experts * capacity + ranks
    )
    back_table = (slot_iota == back_index[:, None]).astype(jnp.bfloat16)
    repeated = jnp.repeat(expert_input, top_count, axis=0)
    outgoing = lax.dot_general(
        send_table, repeated, (((0,), (0,)), ((), ())), preferred_element_type=jnp.float32
    ).astype(jnp.bfloat16)
    outgoing = outgoing.reshape(ep_count, local_experts, capacity, feature_local)
    arrived = lax.all_to_all(outgoing, "ep", split_axis=0, concat_axis=2, tiled=True)
    arrived = arrived.reshape(local_experts * slot_rows, feature_local)
    mix_weights = (gate_b_weight[None], gate_c_weight[None], value_weight[None])
    expert_weights = (expert_gate, expert_up)
    pieces = side_by_side((mix_input, arrived), "tp", 1, 0)
    mix_carry = project_piece(pieces[0], mix_gain, mix_weights, 1)
    expert_carry = project_piece(pieces[1], expert_gain, expert_weights, local_experts)
    mix_totals, mix_squares = mix_carry
    mix_factor = lax.rsqrt(mix_squares / model_width + epsilon)[:, None]
    outer_gate = mix_totals[0][0] * mix_factor
    product = mix_totals[1][0] * mix_factor * (mix_totals[2][0] * mix_factor)
    edge_rows = passed_along(product[mix_rows - 2 :], "ep", 1)
    padded = jnp.concatenate([edge_rows, product], axis=0)
    convolved = (
        conv_weight[0] * padded[:mix_rows]
        + conv_weight[1] * padded[1 : mix_rows + 1]
        + conv_weight[2] * padded[2:]
    )
    gated = (outer_gate * convolved).astype(jnp.bfloat16)
    expert_totals, expert_squares = expert_carry
    expert_factor = lax.rsqrt(expert_squares / model_width + epsilon).reshape(
        local_experts, slot_rows, 1
    )
    activated = (
        jax.nn.silu(expert_totals[0] * expert_factor) * (expert_totals[1] * expert_factor)
    ).astype(jnp.bfloat16)
    summed = jnp.einsum("gsf,gfd->dgs", activated, expert_down, preferred_element_type=jnp.float32)
    summed_all = lax.psum_scatter(
        jnp.concatenate(
            [
                lax.dot_general(
                    out_weight, gated, (((0,), (1,)), ((), ())), preferred_element_type=jnp.float32
                ),
                summed.reshape(lax.axis_size("tp") * feature_local, local_experts * slot_rows),
            ],
            axis=1,
        ).astype(jnp.bfloat16),
        "tp",
        scatter_dimension=0,
        tiled=True,
    ).astype(jnp.float32)
    mix_sum = summed_all[:, :mix_rows]
    expert_sum = summed_all[:, mix_rows:]
    mix_output = mix_sum.T.astype(jnp.bfloat16)
    returning = expert_sum.astype(jnp.bfloat16).reshape(
        feature_local, local_experts, ep_count, capacity
    )
    returned = lax.all_to_all(returning, "ep", split_axis=2, concat_axis=2, tiled=True)
    returned = returned.reshape(feature_local, local_experts * slot_rows)
    picked = lax.dot_general(
        returned, back_table, (((1,), (1,)), ((), ())), preferred_element_type=jnp.float32
    ).reshape(feature_local, tok_local, top_count)
    normalized = route_weight / jnp.sum(route_weight, axis=1, keepdims=True) * routed_scale
    expert_output = jnp.sum(picked * normalized[None], axis=2).T.astype(jnp.bfloat16)
    return (mix_output, expert_output)


def solution(mesh):
    in_specs = (
        P("ep", "tp"),
        P(),
        P(None, "tp"),
        P(None, "tp"),
        P(None, "tp"),
        P(None, "tp"),
        P("tp", None),
        P("ep", "tp"),
        P(),
        P("ep", None),
        P("ep", None),
        P("ep", None, "tp"),
        P("ep", None, "tp"),
        P("ep", "tp", None),
    )
    out_specs = (P("ep", "tp"), P("ep", "tp"))
    return jax.shard_map(local, mesh=mesh, in_specs=in_specs, out_specs=out_specs, check_vma=False)
```

profile of v0, /device:TPU:1, one launch (start us, length us, event | category | flops | bytes accessed | tf_op | source)
XLA Modules:
  0.0 207.0 jit_solution(15245907793472791437)
XLA Ops:
  7.2 0.8 copy.22
  8.3 0.9 reduce-window.6
  9.5 0.8 broadcast_in_dim.2
  11.0 23.6 %all_to_all.14 = bf16[32,1,20,128]{3,2,1,0:T(8,128)(2,1)S(1)} all-to-all(bf16[32,1,20,128]{3,2,1,0:T(8,128)(2,1)S(1)} %bitcast.53), channel_id=1, replica_groups=mesh['ep'=32,'tp'=16] {'ep'}, dimensions={0} | all-to-all | bytes 327680 | tf_op jit(solution)/shard_map/all_to_all | solution.py:81
  34.6 1.6 pad_maximum_fusion.1
  36.3 0.8 slice_bitcast_fusion.2
  37.1 49.4 %all-gather.2.cloned.1.call-done = bf16[1024,2048]{1,0:T(8,128)(2,1)} async-done(((bf16[1024,128]{1,0:T(8,128)(2,1)}), bf16[1024,2048]{1,0:T(8,128)(2,1)}) %all-gather.2.cloned.1.call-update) | async-done | bytes 4194320 | tf_op jit(solution)/shard_map/all_gather | solution.py:12
  86.5 2.5 %fusion.1 = f32[640]{0:T(1024)S(1)} fusion(bf16[1024,2048]{1,0:T(8,128)(2,1)} %all-gather.2.cloned.1.call-done), kind=kLoop, calls=%fused_computation.3 | loop fusion | flops 3931520 | bytes 2624000 | tf_op jit(solution)/shard_map/reduce_sum | solution.py:36
  89.0 1.8 fusion.3
  92.1 0.7 copy-done.3
  92.8 2.1 %collective-permute-start = (f32[2,128]{1,0:T(2,128)S(1)}, f32[2,128]{1,0:T(2,128)S(1)}, u32[]{:S(2)}, u32[]{:S(2)}) collective-permute-start(f32[2,128]{1,0:T(2,128)S(1)} %slice.57), channel_id=1, source_target_pairs={{0,16},{16,32},{32,48},{48,64},{64,80},{80,96},{96,112},{112,128},... | collective-permute-start | bytes 3080 | tf_op jit(solution)/shard_map/ppermute | solution.py:22
  94.9 1.8 fusion.10
  96.8 4.2 %fusion.4 = bf16[2048,640]{0,1:T(8,128)(2,1)S(1)} fusion(f32[2048]{0:T(1024)S(1)} %copy-done.7, bf16[1024,2048]{1,0:T(8,128)(2,1)} %all-gather.2.cloned.1.call-done, bf16[1,192,2048]{2,1,0:T(8,128)(2,1)S(1)} %copy-done, bf16[1,2048,192]{1,2,0:T(8,128)(2,1)} %param.26, f32[640,192]{0,1:T(8,128)} %fusion.10, f32[640]{0:T(1024)S(1)} %add_rsqrt_fusion), kind=kOutput, calls=%fused_computation.10 | convolution fusion | flops 1012736000 | bytes 7318016 | tf_op jit(solution)/shard_map/gsf,gfd->dgs/dot_general | solution.py:107
  101.0 4.8 %fusion.5 = bf16[2048,384]{0,1:T(8,128)(2,1)} fusion(bf16[128,2048]{1,0:T(8,128)(2,1)} %param.20, f32[2,128]{1,0:T(2,128)S(1)} %collective-permute-done, f32[384,128]{1,0:T(8,128)} %copy-done.3, bf16[2048,128]{1,0:T(8,128)(2,1)} %param.16, f32[2048]{0:T(1024)S(1)} %copy-done.8, bf16[1024,2048]{1,0:T(8,128)(2,1)} %all-gather.2.cloned.1.call-done, ...), kind=kOutput, calls=%fused_computation.12 | convolution fusion | flops 406290432 | bytes 4403200 | tf_op jit(solution)/shard_map/dot_general | solution.py:111
  105.9 3.8 %pad_maximum_fusion = bf16[2048,1024]{0,1:T(8,128)(2,1)} fusion(bf16[2048,640]{0,1:T(8,128)(2,1)S(1)} %fusion.4, bf16[2048,384]{0,1:T(8,128)(2,1)} %fusion.5), kind=kLoop, calls=%fused_computation.4 | loop fusion | flops 8388608 | bytes 8388608 | tf_op jit(solution)/shard_map/concatenate | solution.py:109
  109.7 6.4 %copy.31 = bf16[2048,1024]{1,0:T(8,128)(2,1)} copy(bf16[2048,1024]{0,1:T(8,128)(2,1)} %pad_maximum_fusion) | data formatting | bytes 8388608
  116.1 62.3 %reduce-scatter.4.cloned.1.call-done = bf16[128,1024]{1,0:T(8,128)(2,1)} async-done(((bf16[2048,1024]{1,0:T(8,128)(2,1)}), bf16[128,1024]{1,0:T(8,128)(2,1)}) %reduce-scatter.4.cloned.1.call-update) | async-done | bytes 262160
  178.4 0.9 slice.62
  179.5 0.7 reshape.164
  180.3 9.1 %all-to-all-start.1 = ((bf16[128,1,32,20]{0,3,1,2:T(8,128)(2,1)}), bf16[128,1,32,20]{0,3,1,2:T(8,128)(2,1)S(1)}, u32[]{:S(2)}, u32[]{:S(2)}) async-start(bf16[128,1,32,20]{0,3,1,2:T(8,128)(2,1)} %bitcast.12), calls=%async_computation.1 | async-start | bytes 393216 | tf_op jit(solution)/shard_map/all_to_all | solution.py:128
  189.8 0.9 slice.61
  190.7 0.8 copy.33
  191.5 7.8 %all-to-all-done.1 = bf16[128,1,32,20]{0,3,1,2:T(8,128)(2,1)S(1)} async-done(((bf16[128,1,32,20]{0,3,1,2:T(8,128)(2,1)}), bf16[128,1,32,20]{0,3,1,2:T(8,128)(2,1)S(1)}, u32[]{:S(2)}, u32[]{:S(2)}) %all-to-all-start.1) | async-done | bytes 163872 | tf_op jit(solution)/shard_map/all_to_all | solution.py:128
  199.3 0.9 fusion.25
  (44 shorter events, 3.2 us)
Async XLA Ops:
  7.2 89.6 %copy-start = (bf16[1,192,2048]{2,1,0:T(8,128)(2,1)S(1)}, bf16[1,192,2048]{2,1,0:T(8,128)(2,1)}, u32[]{:S(2)}) copy-start(bf16[1,192,2048]{2,1,0:T(8,128)(2,1)} %param.27) | copy-start | bytes 2359300
  7.2 79.3 %all-gather.2.cloned.1.call-start = ((), (), s32[]{:S(2)}) async-start(), calls=%async_computation.3 | async-start | bytes 4456448 | tf_op jit(solution)/shard_map/all_gather | solution.py:12
  10.9 80.0 %copy-start.5 = (bf16[2048,128]{1,0:T(8,128)(2,1)S(1)}, bf16[2048,128]{1,0:T(8,128)(2,1)}, u32[]{:S(2)}) copy-start(bf16[2048,128]{1,0:T(8,128)(2,1)} %param.17) | copy-start | bytes 1572868
  10.9 79.9 %copy-start.8 = (f32[2048]{0:T(1024)S(1)}, f32[2048]{0:T(1024)}, u32[]{:S(2)}) copy-start(f32[2048]{0:T(1024)} %param.15) | copy-start | bytes 24580
  36.2 142.2 %reduce-scatter.4.cloned.1.call-start = ((), (), s32[]{:S(2)}) async-start(), calls=%async_computation.4 | async-start | bytes 4456448
  86.5 4.4 %copy-start.1 = (bf16[1024,2048]{1,0:T(8,128)(2,1)S(1)}, bf16[1024,2048]{1,0:T(8,128)(2,1)}, u32[]{:S(2)}) copy-start(bf16[1024,2048]{1,0:T(8,128)(2,1)} %all-gather.2.cloned.1.call-done) | copy-start | bytes 12582916
  89.0 2.5 %copy-start.6 = (bf16[2048,128]{1,0:T(8,128)(2,1)S(1)}, bf16[2048,128]{1,0:T(8,128)(2,1)}, u32[]{:S(2)}) copy-start(bf16[2048,128]{1,0:T(8,128)(2,1)} %param.18) | copy-start | bytes 1572868
  90.9 4.0 %copy-start.4 = (bf16[1,2048,192]{1,2,0:T(8,128)(2,1)S(1)}, bf16[1,2048,192]{1,2,0:T(8,128)(2,1)}, u32[]{:S(2)}) copy-start(bf16[1,2048,192]{1,2,0:T(8,128)(2,1)} %param.25) | copy-start | bytes 2359300
  90.9 4.0 %copy-start.7 = (f32[2048]{0:T(1024)S(1)}, f32[2048]{0:T(1024)}, u32[]{:S(2)}) copy-start(f32[2048]{0:T(1024)} %param.22) | copy-start | bytes 24580
  92.1 0.7 copy-start.3
  92.8 8.3 %collective-permute-start = (f32[2,128]{1,0:T(2,128)S(1)}, f32[2,128]{1,0:T(2,128)S(1)}, u32[]{:S(2)}, u32[]{:S(2)}) collective-permute-start(f32[2,128]{1,0:T(2,128)S(1)} %slice.57), channel_id=1, source_target_pairs={{0,16},{16,32},{32,48},{48,64},{64,80},{80,96},{96,112},{112,128},... | collective-permute-start | bytes 3080 | tf_op jit(solution)/shard_map/ppermute | solution.py:22
  116.1 73.7 %copy-start.2 = (f32[160,2]{0,1:T(2,128)S(1)}, f32[160,2]{0,1:T(2,128)}, u32[]{:S(2)}) copy-start(f32[160,2]{0,1:T(2,128)} %param.24) | copy-start | bytes 3844
  180.3 19.0 %all-to-all-start.1 = ((bf16[128,1,32,20]{0,3,1,2:T(8,128)(2,1)}), bf16[128,1,32,20]{0,3,1,2:T(8,128)(2,1)S(1)}, u32[]{:S(2)}, u32[]{:S(2)}) async-start(bf16[128,1,32,20]{0,3,1,2:T(8,128)(2,1)} %bitcast.12), calls=%async_computation.1 | async-start | bytes 393216 | tf_op jit(solution)/shard_map/all_to_all | solution.py:128
Sparse Core Ops, SparseCore 0:
  36.4 50.0 all-gather.1
  116.2 62.1 reduce-scatter.3
where the time goes:
time: 210 us; the launch traced here: 207 us
  waiting for transfers between devices  120 us (57%)
  blocking collectives  23.6 us (11%)
  between operations  14.3 us (7%)
  local copies, waits for them, and re-layouts  13.8 us (7%)
  matrix products  13.5 us (6%)
  starting transfers between devices  11.3 us (5%)
  other arithmetic  11 us (5%)
    unnamed x3, waiting for transfers between devices  62.4 us
    all_gather x1, waiting for transfers between devices, side_by_side(): out, at, done = (lax.all_gather(both, axis, axis=dim, tiled=True), 0, [])  49.4 us
    all_to_all x1, blocking collectives, local(): lax.all_to_all(outgoing, 'ep', split_axis=0, concat_axis=2, tiled=True)  23.6 us
    all_to_all x1, starting transfers between devices, local(): lax.all_to_all(returning, 'ep', split_axis=2, concat_axis=2, tiled=True)  9.08 us
    unnamed x22, local copies, waits for them, and re-layouts  8.89 us
    all_to_all x1, waiting for transfers between devices, local(): lax.all_to_all(returning, 'ep', split_axis=2, concat_axis=2, tiled=True)  7.75 us
    dot_general x1, matrix products, local(): lax.dot_general(out_weight, gated, (((0,), (1,)), ((), ())), preferred_el...  4.83 us
    reduce_sum x2, other arithmetic, project_piece(): return (updated, jnp.sum(widened * widened, axis=-1))  4.32 us
  transfers between devices with their start and end apart: 4, of which 3 were waited for; matrix products, arithmetic and copies ran while one was open for 4% of the time, Pallas kernels for 0%

commit v1 on v0

v1 whole, which is shorter than its diff:
```python
import functools

import jax
import jax.numpy as jnp
from jax import lax
from jax.experimental import pallas as pl
from jax.experimental.pallas import tpu as pltpu
from jax.sharding import PartitionSpec as P

epsilon = 1e-06
routed_scale = 2.5
MESH = pl.DeviceIdType.MESH
F32 = jnp.float32
BF16 = jnp.bfloat16
L = 128
W = 2 * L


def mm(a, b):
    return jnp.dot(a, b, preferred_element_type=F32)


def mm_nt(a, b):
    return lax.dot_general(a, b, (((1,), (1,)), ((), ())), preferred_element_type=F32)


def kernel(
    n_ep,
    n_y,
    cap,
    stride,
    mix_in,
    mix_gain,
    gb,
    gc,
    vw,
    cw,
    ow,
    ex_in,
    ex_gain,
    routes,
    scores,
    eg,
    eu,
    ed,
    mix_out,
    ex_out,
    xm,
    xe,
    xsm,
    xse,
    ssm,
    sse,
    wm,
    wo,
    wg,
    wu,
    wd,
    wc,
    rt,
    tpad,
    xpad,
    dsend,
    rbuf,
    prod,
    outer,
    gated,
    act,
    rs_m_send,
    rs_m_recv,
    rs_e_send,
    rs_e_recv,
    ymo,
    ysend,
    rsend,
    ret,
    ag_sem_m,
    ag_sem_e,
    rs_sem_m,
    rs_sem_e,
    d_send,
    d_recv,
    r_send,
    r_recv,
    w_local,
    w_send,
    w_recv,
    misc,
):
    ep = lax.axis_index("ep")
    tp = lax.axis_index("tp")
    y, c = tp // 2, lax.rem(tp, 2)
    o = 1 - c
    partner = 2 * y + o
    half_ep = n_ep // 2
    hs = ep // half_ep
    lm = ep - hs * half_ep
    long, short = n_y // 2, n_y - 1 - n_y // 2
    ring_tp = (2 * lax.rem(y + n_y - 1, n_y) + c, 2 * lax.rem(y + 1, n_y) + c)
    sign = (1, -1)
    rows_m = xm.shape[1]
    rows_e = xe.shape[1]
    hid = wg.shape[0] // 2

    barrier = pltpu.get_barrier_semaphore()

    def greet(j, carry):
        e = lax.rem(ep + j, n_ep)
        pl.semaphore_signal(barrier, inc=1, device_id=(e, 2 * y), device_id_type=MESH)
        pl.semaphore_signal(barrier, inc=1, device_id=(e, 2 * y + 1), device_id_type=MESH)
        return carry

    for t in ring_tp:
        pl.semaphore_signal(barrier, inc=1, device_id=(ep, t), device_id_type=MESH)
    pl.semaphore_signal(barrier, inc=1, device_id=(ep, partner), device_id_type=MESH)
    lax.fori_loop(1, n_ep, greet, 0)

    def lanes(who, base=0):
        return pl.ds(pl.multiple_of(base + who * L, L), L)

    def weight_slots(who):
        return (
            (gb, wm.at[:, lanes(who)]),
            (gc, wm.at[:, lanes(who, W)]),
            (vw, wm.at[:, lanes(who, 2 * W)]),
            (cw, wc.at[who]),
            (ow, wo.at[pl.ds(pl.multiple_of(who * L, L), L)]),
            (eg, wg.at[pl.ds(pl.multiple_of(who * hid, hid), hid)]),
            (eu, wu.at[pl.ds(pl.multiple_of(who * hid, hid), hid)]),
            (ed, wd.at[pl.ds(pl.multiple_of(who * hid, hid), hid)]),
        )

    def mix_half(who):
        return mix_in.at[pl.ds(pl.multiple_of(who * rows_m, rows_m), rows_m)]

    own_mix = pltpu.make_async_copy(mix_half(c), xm.at[y, :, lanes(c)], misc.at[0])
    own_mix.start()
    own_weights = [
        pltpu.make_async_copy(src, dst, w_local.at[i])
        for i, (src, dst) in enumerate(weight_slots(c))
    ]
    for copy in own_weights:
        copy.start()

    tok, top = ex_in.shape[0], routes.shape[0]
    slots_all = n_ep * stride
    rt[...] = jnp.full(rt.shape, -1, jnp.int32)
    rt[0:top, 0:tok] = routes[...]
    tpad[...] = jnp.zeros_like(tpad)
    total_score = scores[0:1, :] + scores[1:2, :]
    tpad[2:3, 0:tok] = scores[0:1, :] / total_score * routed_scale
    tpad[3:4, 0:tok] = scores[1:2, :] / total_score * routed_scale
    xpad[...] = jnp.zeros_like(xpad)
    xpad[0:tok, :] = ex_in[...]
    tokens = rt.shape[1]
    experts = lax.broadcasted_iota(jnp.int32, (n_ep, tokens), 0)
    hit = [experts == rt[k : k + 1, :] for k in range(top)]
    ones = [h.astype(F32) for h in hit]
    before = (
        lax.broadcasted_iota(jnp.int32, (tokens, tokens), 0)
        < lax.broadcasted_iota(jnp.int32, (tokens, tokens), 1)
    ).astype(F32)
    ranks = mm((ones[0] + ones[1]).astype(BF16), before.astype(BF16))
    rows_iota = lax.broadcasted_iota(jnp.int32, (slots_all, tokens), 0)
    table = None
    for k in range(top):
        rank = jnp.sum(ranks * ones[k], axis=0, keepdims=True)
        slot = rt[k : k + 1, :] * stride + rank.astype(jnp.int32)
        tpad[k : k + 1, :] = slot.astype(F32)
        here = rows_iota == slot
        table = here if table is None else table | here
    outgoing = mm(table.astype(F32).astype(BF16), xpad[...]).astype(BF16)
    dsend[...] = outgoing.reshape(dsend.shape)

    pl.semaphore_wait(barrier, 2 * (n_ep - 1) + 3)

    give_mix = pltpu.make_async_remote_copy(
        src_ref=mix_half(o),
        dst_ref=xm.at[y, :, lanes(c)],
        send_sem=misc.at[1],
        recv_sem=misc.at[2],
        device_id=(ep, partner),
        device_id_type=MESH,
    )
    give_mix.start()

    def dispatch_copy(e):
        return pltpu.make_async_remote_copy(
            src_ref=dsend.at[e],
            dst_ref=rbuf.at[c, lm],
            send_sem=d_send.at[e],
            recv_sem=d_recv.at[c * half_ep + lm],
            device_id=(e, 2 * y + hs),
            device_id_type=MESH,
        )

    def dispatch(j, carry):
        dispatch_copy(lax.rem(ep + j, n_ep)).start()
        return carry

    @pl.when(c == hs)
    def _():
        rbuf[c, lm] = dsend[ep]

    @pl.when(c != hs)
    def _():
        dispatch_copy(ep).start()

    lax.fori_loop(1, n_ep, dispatch, 0)

    give_weights = [
        pltpu.make_async_remote_copy(
            src_ref=src,
            dst_ref=dst,
            send_sem=w_send.at[i],
            recv_sem=w_recv.at[i],
            device_id=(ep, partner),
            device_id_type=MESH,
        )
        for i, (src, dst) in enumerate(weight_slots(c))
    ]
    for copy in give_weights:
        copy.start()

    def hops(way, part):
        return long if way == part else short

    def gather_copy(x, sem, way, part, step):
        half = x.shape[1] // 2
        origin = lax.rem(y + sign[way] * step + n_y, n_y)
        block = x.at[origin, pl.ds(part * half, half)]
        return pltpu.make_async_remote_copy(
            src_ref=block,
            dst_ref=block,
            send_sem=sem.at[0, way, part, step],
            recv_sem=sem.at[1, way, part, step],
            device_id=(ep, ring_tp[way]),
            device_id_type=MESH,
        )

    def gather_arrived(x, sem, way, part, step):
        half = x.shape[1] // 2
        origin = lax.rem(y + sign[way] * (step + 1) + n_y, n_y)
        block = x.at[origin, pl.ds(part * half, half)]
        pltpu.make_async_remote_copy(
            src_ref=block,
            dst_ref=block,
            send_sem=sem.at[0, way, part, step],
            recv_sem=sem.at[1, way, part, step],
            device_id=(ep, ring_tp[way]),
            device_id_type=MESH,
        ).wait_recv()

    def gather_start(x, sem):
        for part in range(2):
            for way in range(2):
                if hops(way, part) > 0:
                    gather_copy(x, sem, way, part, 0).start()

    def gather_step(x, sem, step):
        for way in range(2):
            for part in (way, 1 - way):
                if step < hops(way, part):
                    gather_arrived(x, sem, way, part, step)
                    if step + 1 < hops(way, part):
                        gather_copy(x, sem, way, part, step + 1).start()

    def gather_end(x, sem):
        for way in range(2):
            for part in range(2):
                for step in range(hops(way, part)):
                    gather_copy(x, sem, way, part, step).wait_send()

    def scale(x, xs, ss, gain, origin):
        cols = pl.ds(pl.multiple_of(origin * W, W), W)
        wide = x[origin].astype(F32)
        square = wide * wide
        ss[...] += square[:, :L] + square[:, L:]
        xs[:, cols] = (wide * gain[:, cols]).astype(BF16)

    def scale_step(x, xs, ss, gain, step):
        scale(x, xs, ss, gain, lax.rem(y + step + 1, n_y))
        if step < long - 1:
            scale(x, xs, ss, gain, lax.rem(y - step - 1 + n_y, n_y))

    def factor_of(ss):
        return lax.rsqrt(jnp.sum(ss[...], axis=1, keepdims=True) / (n_y * W) + epsilon)

    mix = (xm, ag_sem_m)
    exp = (xe, ag_sem_e)
    mix_scale = (xm, xsm, ssm, mix_gain)
    exp_scale = (xe, xse, sse, ex_gain)

    ssm[...] = jnp.zeros_like(ssm)
    sse[...] = jnp.zeros_like(sse)
    own_mix.wait()
    give_mix.wait_recv()
    gather_start(*mix)
    scale(*mix_scale, y)

    def take_dispatch():
        def one(l, carry):
            for cs in range(2):

                @pl.when(jnp.logical_not((c * half_ep + l == ep) & (c == cs)))
                def _():
                    pltpu.make_async_remote_copy(
                        src_ref=rbuf.at[cs, l],
                        dst_ref=rbuf.at[cs, l],
                        send_sem=d_send.at[l],
                        recv_sem=d_recv.at[cs * half_ep + l],
                        device_id=(ep, partner),
                        device_id_type=MESH,
                    ).wait_recv()

            return carry

        lax.fori_loop(0, half_ep, one, 0)
        wide = half_ep * stride
        row = lax.broadcasted_iota(jnp.int32, (rows_e, wide), 0)
        col = lax.broadcasted_iota(jnp.int32, (rows_e, wide), 1)
        group = (row * (65536 // cap + 1)) >> 16
        pick = (col - row == group * (stride - cap)).astype(F32).astype(BF16)
        for cs in range(2):
            part = rbuf[cs].reshape(wide, L)
            xe[y, :, cs * L : cs * L + L] = mm(pick, part).astype(BF16)
        gather_start(*exp)
        scale(*exp_scale, y)

    def sum_copy(send, recv, sem, way, part, step):
        return pltpu.make_async_remote_copy(
            src_ref=send.at[way, part, step],
            dst_ref=recv.at[way, part, step],
            send_sem=sem.at[0, way, part, step],
            recv_sem=sem.at[1, way, part, step],
            device_id=(ep, ring_tp[way]),
            device_id_type=MESH,
        )

    def partial_sum(left, right, dest, part):
        half = left.shape[0] // 2
        cols = pl.ds(pl.multiple_of(dest * W, W), W)
        return mm(left[part * half : part * half + half], right[:, cols])

    def sum_step(left, right, send, recv, sem, step):
        for way in range(2):
            dest = lax.rem(y - sign[way] * (long - step) + n_y, n_y)
            for part in (way, 1 - way):
                first = long - hops(way, part)
                if step < first:
                    continue
                value = partial_sum(left, right, dest, part)
                if step > first:
                    sum_copy(send, recv, sem, way, part, step - 1).wait_recv()
                    value = value + recv[way, part, step - 1].astype(F32)
                send[way, part, step] = value.astype(BF16)
                sum_copy(send, recv, sem, way, part, step).start()

    def sum_result(left, right, send, recv, sem, part):
        value = partial_sum(left, right, y, part)
        for way in range(2):
            if hops(way, part) > 0:
                sum_copy(send, recv, sem, way, part, long - 1).wait_recv()
                value = value + recv[way, part, long - 1].astype(F32)
        return value.astype(BF16)

    def sum_end(left, right, send, recv, sem):
        for way in range(2):
            for part in range(2):
                for step in range(long - hops(way, part), long):
                    sum_copy(send, recv, sem, way, part, step).wait_send()

    mix_sum = (gated, wo, rs_m_send, rs_m_recv, rs_sem_m)
    exp_sum = (act, wd, rs_e_send, rs_e_recv, rs_sem_e)

    def take_weights(lo, hi):
        for i in range(lo, hi):
            own_weights[i].wait()
            give_weights[i].wait_recv()

    next_ep = jnp.where(c == 0, ep, ep + 1)
    halo = pltpu.make_async_remote_copy(
        src_ref=prod.at[pl.ds(rows_m, 8)],
        dst_ref=prod.at[pl.ds(0, 8)],
        send_sem=misc.at[3],
        recv_sem=misc.at[4],
        device_id=(lax.rem(next_ep, n_ep), partner),
        device_id_type=MESH,
    )
    has_next = jnp.logical_not((c == 1) & (ep == n_ep - 1))
    has_last = jnp.logical_not((c == 0) & (ep == 0))

    def mixer_project():
        factor = factor_of(ssm)
        take_weights(0, 4)
        inner = mm(xsm[...], wm[:, W : 2 * W]) * factor
        values = mm(xsm[...], wm[:, 2 * W :]) * factor
        prod[pl.ds(8, rows_m), :] = inner * values

        @pl.when(has_next)
        def _():
            halo.start()

        outer[...] = mm(xsm[...], wm[:, :W]) * factor

    def mixer_convolve():
        @pl.when(has_last)
        def _():
            halo.wait_recv()

        @pl.when(jnp.logical_not(has_last))
        def _():
            prod[0:8, :] = jnp.zeros((8, W), F32)

        for part in range(2):
            cols = slice(part * L, part * L + L)
            convolved = (
                wc[part, 0:1] * prod[pl.ds(6, rows_m), cols]
                + wc[part, 1:2] * prod[pl.ds(7, rows_m), cols]
                + wc[part, 2:3] * prod[pl.ds(8, rows_m), cols]
            )
            gated[:, cols] = (outer[:, cols] * convolved).astype(BF16)
        take_weights(4, 5)

    def expert_hidden():
        factor = factor_of(sse)
        take_weights(5, 8)
        gate = mm_nt(xse[...], wg[...]) * factor
        up = mm_nt(xse[...], wu[...]) * factor
        act[...] = (gate / (1.0 + jnp.exp(-gate)) * up).astype(BF16)

    give_out = pltpu.make_async_remote_copy(
        src_ref=ysend,
        dst_ref=ymo.at[pl.ds(pl.multiple_of(c * rows_m, rows_m), rows_m)],
        send_sem=misc.at[5],
        recv_sem=misc.at[6],
        device_id=(ep, partner),
        device_id_type=MESH,
    )

    def mixer_result():
        half = rows_m // 2
        for part in range(2):
            value = sum_result(*mix_sum, part)
            left, right = value[:, :L], value[:, L:]
            mine = jnp.where(c == 0, left, right)
            theirs = jnp.where(c == 0, right, left)
            ymo[pl.ds(pl.multiple_of(c * rows_m + part * half, half), half), :] = mine
            ysend[part * half : part * half + half] = theirs
        give_out.start()

    def return_copy(l, cs):
        return pltpu.make_async_remote_copy(
            src_ref=rsend.at[cs, l],
            dst_ref=ret.at[ep],
            send_sem=r_send.at[cs * half_ep + l],
            recv_sem=r_recv.at[ep],
            device_id=(c * half_ep + l, 2 * y + cs),
            device_id_type=MESH,
        )

    def is_self(l, cs):
        return (c * half_ep + l == ep) & (c == cs)

    def return_part(part):
        value = sum_result(*exp_sum, part)
        groups = half_ep // 2
        slots = groups * stride
        row = lax.broadcasted_iota(jnp.int32, (slots, rows_e // 2), 0)
        col = lax.broadcasted_iota(jnp.int32, (slots, rows_e // 2), 1)
        group = (col * (65536 // cap + 1)) >> 16
        pick = (row - col == group * (stride - cap)).astype(F32).astype(BF16)
        spread = mm(pick, value).astype(BF16)
        for cs in range(2):
            piece = spread[:, cs * L : cs * L + L].reshape(groups, stride, L)
            rsend[cs, part * groups : part * groups + groups] = piece

        def one(i, carry):
            l = part * groups + lax.rem(ep + i, groups)
            for cs in range(2):

                @pl.when(jnp.logical_not(is_self(l, cs)))
                def _():
                    return_copy(l, cs).start()

            return carry

        lax.fori_loop(0, groups, one, 0)

    early = min(2, long)
    for step in range(early):
        gather_step(*mix, step)
        scale_step(*mix_scale, step)
    take_dispatch()
    for step in range(early, long):
        gather_step(*mix, step)
        scale_step(*mix_scale, step)
        gather_step(*exp, step - early)
        scale_step(*exp_scale, step - early)
    mixer_project()
    rest = list(range(long - early, long))
    gather_step(*exp, rest[0])
    scale_step(*exp_scale, rest[0])
    mixer_convolve()
    sum_step(*mix_sum, 0)
    for step in rest[1:]:
        gather_step(*exp, step)
        scale_step(*exp_scale, step)
    if long > 1:
        sum_step(*mix_sum, 1)
    expert_hidden()
    for step in range(long):
        sum_step(*exp_sum, step)
        if step + 2 < long:
            sum_step(*mix_sum, step + 2)
    mixer_result()
    for part in range(2):
        return_part(part)

    @pl.when(c == hs)
    def _():
        ret[ep] = rsend[c, lm]

    give_out.wait_recv()
    out_copy = pltpu.make_async_copy(ymo, mix_out, misc.at[7])
    out_copy.start()

    tcol = jnp.transpose(tpad[...])
    lane = lax.broadcasted_iota(jnp.int32, (tok, slots_all), 1)

    def take_return(e, carry):
        @pl.when(jnp.logical_not((e == ep) & (hs == c)))
        def _():
            pltpu.make_async_remote_copy(
                src_ref=ret.at[e],
                dst_ref=ret.at[e],
                send_sem=r_send.at[e],
                recv_sem=r_recv.at[e],
                device_id=(ep, partner),
                device_id_type=MESH,
            ).wait_recv()

        return carry

    lax.fori_loop(0, n_ep, take_return, 0)
    back = ret[...].reshape(slots_all, L)
    total = None
    for k in range(top):
        pick = (lane == tcol[0:tok, k : k + 1].astype(jnp.int32)).astype(F32).astype(BF16)
        term = mm(pick, back) * tcol[0:tok, 2 + k : 3 + k]
        total = term if total is None else total + term
    ex_out[...] = total.astype(BF16)

    def dispatched(j, carry):
        dispatch_copy(lax.rem(ep + j, n_ep)).wait_send()
        return carry

    lax.fori_loop(1, n_ep, dispatched, 0)

    @pl.when(c != hs)
    def _():
        dispatch_copy(ep).wait_send()

    def returned(l, carry):
        for cs in range(2):

            @pl.when(jnp.logical_not(is_self(l, cs)))
            def _():
                return_copy(l, cs).wait_send()

        return carry

    lax.fori_loop(0, half_ep, returned, 0)
    give_mix.wait_send()
    for copy in give_weights:
        copy.wait_send()

    @pl.when(has_next)
    def _():
        halo.wait_send()

    give_out.wait_send()
    gather_end(*mix)
    gather_end(*exp)
    sum_end(*mix_sum)
    sum_end(*exp_sum)
    out_copy.wait()


def local(
    mix_input,
    mix_gain,
    gate_b_weight,
    gate_c_weight,
    value_weight,
    conv_weight,
    out_weight,
    expert_input,
    expert_gain,
    routes,
    route_weight,
    expert_gate,
    expert_up,
    expert_down,
):
    n_ep, n_tp = lax.axis_size("ep"), lax.axis_size("tp")
    n_y = n_tp // 2
    tok, top = routes.shape
    cap = 2 * tok * top // n_ep
    stride = -(-cap // 8) * 8
    half_ep = n_ep // 2
    rows_m = mix_input.shape[0] // 2
    rows_e = half_ep * cap
    width = mix_gain.shape[0]
    hid = expert_gate.shape[2]
    tokens = -(-tok // L) * L
    long = n_y // 2
    slots_all = n_ep * stride
    dma = pltpu.SemaphoreType.DMA
    any_spec = pl.BlockSpec(memory_space=pl.ANY)
    vmem = pl.BlockSpec(memory_space=pltpu.VMEM)
    scratch = [
        pltpu.VMEM((n_y, rows_m, W), BF16),
        pltpu.VMEM((n_y, rows_e, W), BF16),
        pltpu.VMEM((rows_m, width), BF16),
        pltpu.VMEM((rows_e, width), BF16),
        pltpu.VMEM((rows_m, L), F32),
        pltpu.VMEM((rows_e, L), F32),
        pltpu.VMEM((width, 3 * W), BF16),
        pltpu.VMEM((W, width), BF16),
        pltpu.VMEM((2 * hid, width), BF16),
        pltpu.VMEM((2 * hid, width), BF16),
        pltpu.VMEM((2 * hid, width), BF16),
        pltpu.VMEM((2, 3, L), F32),
        pltpu.VMEM((8, tokens), jnp.int32),
        pltpu.VMEM((8, tokens), F32),
        pltpu.VMEM((tokens, L), BF16),
        pltpu.VMEM((n_ep, stride, L), BF16),
        pltpu.VMEM((2, half_ep, stride, L), BF16),
        pltpu.VMEM((8 + rows_m, W), F32),
        pltpu.VMEM((rows_m, W), F32),
        pltpu.VMEM((rows_m, W), BF16),
        pltpu.VMEM((rows_e, 2 * hid), BF16),
        pltpu.VMEM((2, 2, long, rows_m // 2, W), BF16),
        pltpu.VMEM((2, 2, long, rows_m // 2, W), BF16),
        pltpu.VMEM((2, 2, long, rows_e // 2, W), BF16),
        pltpu.VMEM((2, 2, long, rows_e // 2, W), BF16),
        pltpu.VMEM((2 * rows_m, L), BF16),
        pltpu.VMEM((rows_m, L), BF16),
        pltpu.VMEM((2, half_ep, stride, L), BF16),
        pltpu.VMEM((n_ep, stride, L), BF16),
        dma((2, 2, 2, long)),
        dma((2, 2, 2, long)),
        dma((2, 2, 2, long)),
        dma((2, 2, 2, long)),
        dma((n_ep,)),
        dma((n_ep,)),
        dma((n_ep,)),
        dma((n_ep,)),
        dma((8,)),
        dma((8,)),
        dma((8,)),
        dma((8,)),
    ]
    return pl.pallas_call(
        functools.partial(kernel, n_ep, n_y, cap, stride),
        out_shape=(
            jax.ShapeDtypeStruct(mix_input.shape, BF16),
            jax.ShapeDtypeStruct(expert_input.shape, BF16),
        ),
        in_specs=[
            any_spec,
            vmem,
            any_spec,
            any_spec,
            any_spec,
            any_spec,
            any_spec,
            vmem,
            vmem,
            vmem,
            vmem,
            any_spec,
            any_spec,
            any_spec,
        ],
        out_specs=(any_spec, vmem),
        scratch_shapes=scratch,
        compiler_params=pltpu.CompilerParams(
            collective_id=0, has_side_effects=True, vmem_limit_bytes=56 * 1024 * 1024
        ),
    )(
        mix_input,
        mix_gain.reshape(1, width),
        gate_b_weight,
        gate_c_weight,
        value_weight,
        conv_weight,
        out_weight,
        expert_input,
        expert_gain.reshape(1, width),
        routes.T,
        route_weight.T,
        jnp.swapaxes(expert_gate, 1, 2)[0],
        jnp.swapaxes(expert_up, 1, 2)[0],
        expert_down[0],
    )


def solution(mesh):
    in_specs = (
        P("ep", "tp"),
        P(),
        P(None, "tp"),
        P(None, "tp"),
        P(None, "tp"),
        P(None, "tp"),
        P("tp", None),
        P("ep", "tp"),
        P(),
        P("ep", None),
        P("ep", None),
        P("ep", None, "tp"),
        P("ep", None, "tp"),
        P("ep", "tp", None),
    )
    out_specs = (P("ep", "tp"), P("ep", "tp"))
    return jax.shard_map(local, mesh=mesh, in_specs=in_specs, out_specs=out_specs, check_vma=False)
```

time: 210 us -> 85.1 us (0.41); the launches traced: 207 us -> 84.9 us
  waiting for transfers between devices: 120 us -> 0 us
  Pallas kernels: 0 us -> 82.1 us
  blocking collectives: 23.6 us -> 0 us
  between operations: 14.3 us -> 0.65 us
  matrix products: 13.5 us -> 0 us
  local copies, waits for them, and re-layouts: 13.8 us -> 2.17 us
  starting transfers between devices: 11.3 us -> 0 us
  other arithmetic: 11 us -> 0 us
    pallas_call x0 -> x1, Pallas kernels: none -> 82.1 us  [local(): pl.pallas_call(functools.partial(kernel, n_ep, n_y, cap, stride), out_sha...]
    unnamed x3 -> x0, waiting for transfers between devices: 62.4 us -> none
    all_gather x1 -> x0, waiting for transfers between devices: 49.4 us -> none  [side_by_side(): out, at, done = (lax.all_gather(both, axis, axis=dim, tiled=True), 0, [])]
    all_to_all x1 -> x0, blocking collectives: 23.6 us -> none  [local(): lax.all_to_all(outgoing, 'ep', split_axis=0, concat_axis=2, tiled=True)]
    dot_general x7 -> x0, matrix products: 13.5 us -> none  [the longest x1 4.83 us: local(): lax.dot_general(out_weight, gated, (((0,), (1,)), ((), ())), preferred_el...]
    all_to_all x1 -> x0, starting transfers between devices: 9.08 us -> none  [local(): lax.all_to_all(returning, 'ep', split_axis=2, concat_axis=2, tiled=True)]
    all_to_all x1 -> x0, waiting for transfers between devices: 7.75 us -> none  [local(): lax.all_to_all(returning, 'ep', split_axis=2, concat_axis=2, tiled=True)]
    unnamed x22 -> x4, local copies, waits for them, and re-layouts: 8.89 us -> 2.17 us
  transfers between devices with their start and end apart: 4 -> 0, of which waited for: 3 -> 0; matrix products, arithmetic and copies ran while one was open for 4% -> 0% of each run, Pallas kernels for 0% -> 0%
where the time goes in v1:
time: 85.1 us; the launch traced here: 84.9 us
  Pallas kernels  82.1 us (96%)
  local copies, waits for them, and re-layouts  2.17 us (3%)
    pallas_call x1, Pallas kernels, local(): pl.pallas_call(functools.partial(kernel, n_ep, n_y, cap, stride), out_sha...  82.1 us
    unnamed x4, local copies, waits for them, and re-layouts  2.17 us

profile of v1, /device:TPU:1, one launch (start us, length us, event | category | flops | bytes accessed | tf_op | source)
XLA Modules:
  0.0 84.9 jit_solution(13323576175526461777)
XLA Ops:
  0.6 82.1 %shard_map.149 = (bf16[384,128]{1,0:T(8,128)(2,1)}, bf16[160,128]{1,0:T(8,128)(2,1)}) custom-call(bf16[384,128]{1,0:T(8,128)(2,1)} %mix_in.1, f32[1,2048]{1,0:T(1,128)} %bitcast.14, bf16[2048,128]{1,0:T(8,128)(2,1)} %gb.1, bf16[2048,128]{1,0:T(8,128)(2,1)} %gc.1, bf16[2048,128]{1,0:T(8,128)(2,1)} %vw.1, f32[3,128]{1,0:T(4,128)} %cw.1, bf16[128,2048]{1,0:T(8,128)(2,1)} %ow.1, ...), custom_call_target="tpu_custom_call" | custom-call | tf_op jit(solution)/shard_map/pallas_call | solution.py:665
  82.8 0.0 copy-start
  82.8 1.5 %copy.18 = bf16[384,128]{1,0:T(8,128)(2,1)} copy(bf16[384,128]{1,0:T(8,128)(2,1)} %get-tuple-element.4) | data formatting | bytes 196608
  84.3 0.0 copy-done
  84.3 0.6 copy.19
Async XLA Ops:
  82.8 1.6 %copy-start = (bf16[160,128]{1,0:T(8,128)(2,1)S(1)}, bf16[160,128]{1,0:T(8,128)(2,1)}, u32[]{:S(2)}) copy-start(bf16[160,128]{1,0:T(8,128)(2,1)} %get-tuple-element.5) | copy-start | bytes 122884

commit v2 on v1

v2 whole, which is shorter than its diff:
```python
import functools

import jax
import jax.numpy as jnp
from jax import lax
from jax.experimental import pallas as pl
from jax.experimental.pallas import tpu as pltpu
from jax.sharding import PartitionSpec as P

epsilon = 1e-06
routed_scale = 2.5
MESH = pl.DeviceIdType.MESH
F32 = jnp.float32
BF16 = jnp.bfloat16
L = 128
W = 2 * L
PARTS = 4
Z = 2 * PARTS
PLACE = {0: 0, 1: 0, -1: 1, 2: 1, -2: 2, 3: 2, -3: 3, 4: 3}
EVEN, ODD = (0, 2, -2, 4), (1, -1, 3, -3)


def mm(a, b):
    return jnp.dot(a, b, preferred_element_type=F32)


def mm_nt(a, b):
    return lax.dot_general(a, b, (((1,), (1,)), ((), ())), preferred_element_type=F32)


def kernel(
    n_ep,
    n_y,
    cap,
    stride,
    mix_in,
    mix_gain_in,
    gb,
    gc,
    vw,
    cw,
    ow,
    ex_in_in,
    ex_gain_in,
    routes_in,
    scores_in,
    eg,
    eu,
    ed,
    mix_out,
    ex_out,
    mix_gain,
    ex_gain,
    routes,
    scores,
    ex_in,
    ga,
    ua,
    xm,
    xe,
    xsm,
    xse,
    ssm,
    sse,
    wm,
    wo,
    wg,
    wu,
    wd,
    wc,
    rt,
    tpad,
    xpad,
    dsend,
    rbuf,
    prod,
    outer,
    gated,
    act,
    rs_m_send,
    rs_m_recv,
    rs_e_send,
    rs_e_recv,
    ymo,
    ysend,
    rsend,
    ret,
    pre_m,
    pre_e,
    ag_sem_m,
    ag_sem_e,
    rs_sem_m,
    rs_sem_e,
    s_sem,
    d_sem,
    w_local,
    w_send,
    w_recv,
    i_sem,
    misc,
):
    ep = lax.axis_index("ep")
    tp = lax.axis_index("tp")
    y, c = tp // 2, lax.rem(tp, 2)
    o = 1 - c
    partner = 2 * y + o
    half_ep = n_ep // 2
    n_x = n_ep // Z
    z, x_own = ep // n_x, lax.rem(ep, n_x)
    hs = lax.rem(z, 2)
    odd = lax.rem(z + c, 2)
    long, short = n_y // 2, n_y - 1 - n_y // 2
    ring_tp = (2 * lax.rem(y + n_y - 1, n_y) + c, 2 * lax.rem(y + 1, n_y) + c)
    sign = (1, -1)
    rows_m = xm.shape[1]
    rows_e = xe.shape[1]
    hid = wg.shape[0] // 2

    def hops(way, part):
        return long if way == part // (PARTS // 2) else short

    order = [(way, part) for part in range(PARTS) for way in range(2)]
    last_first = [(way, part) for part in reversed(range(PARTS)) for way in range(2)]
    place = {}
    for step in range(long):
        for way, part in order:
            if step < hops(way, part):
                place[way, part, step] = len(place)

    barrier = pltpu.get_barrier_semaphore()

    def along_x(off, body):
        lo = 1 if off == 0 else 0

        def one(j, carry):
            body(lax.rem(z + off + Z, Z) * n_x + lax.rem(x_own + j, n_x))
            return carry

        lax.fori_loop(lo, n_x, one, 0)

    def greet(e):
        pl.semaphore_signal(barrier, inc=1, device_id=(e, 2 * y), device_id_type=MESH)
        pl.semaphore_signal(barrier, inc=1, device_id=(e, 2 * y + 1), device_id_type=MESH)

    for t in ring_tp:
        pl.semaphore_signal(barrier, inc=1, device_id=(ep, t), device_id_type=MESH)
    pl.semaphore_signal(barrier, inc=1, device_id=(ep, partner), device_id_type=MESH)
    for off in sorted(PLACE, key=abs, reverse=True):
        along_x(off, greet)

    small = [
        pltpu.make_async_copy(src, dst, i_sem.at[i])
        for i, (src, dst) in enumerate(
            (
                (routes_in, routes),
                (scores_in, scores),
                (ex_in_in, ex_in),
                (mix_gain_in, mix_gain),
                (ex_gain_in, ex_gain),
            )
        )
    ]
    for copy in small:
        copy.start()
    def lanes(who, base=0):
        return pl.ds(pl.multiple_of(base + who * L, L), L)

    def lane_pieces(src, dst, who, base):
        half = src.shape[0] // 2
        return [
            (src.at[pl.ds(i * half, half)], dst.at[pl.ds(i * half, half), lanes(who, base)])
            for i in range(2)
        ]

    def row_pieces(src, dst, who, count):
        rows = src.shape[0] // count
        return [
            (
                src.at[pl.ds(i * rows, rows)],
                dst.at[pl.ds(pl.multiple_of(who * (rows * count) + i * rows, rows), rows)],
            )
            for i in range(count)
        ]

    def weight_slots(who):
        return (
            (lane_pieces(gb, wm, who, 0), gb, wm.at[:, lanes(who)]),
            (lane_pieces(gc, wm, who, W), gc, wm.at[:, lanes(who)]),
            (lane_pieces(vw, wm, who, 2 * W), vw, wm.at[:, lanes(who)]),
            ([(cw, wc.at[who])], cw, wc.at[who]),
            (row_pieces(eg, wg, who, 3), eg, wg.at[pl.ds(0, hid)]),
            (row_pieces(eu, wu, who, 3), eu, wu.at[pl.ds(0, hid)]),
            (row_pieces(ow, wo, who, 2), ow, wo.at[pl.ds(0, L)]),
            (row_pieces(ed, wd, who, 3), ed, wd.at[pl.ds(0, hid)]),
        )

    def mix_half(who):
        return mix_in.at[pl.ds(pl.multiple_of(who * rows_m, rows_m), rows_m)]

    own_mix = pltpu.make_async_copy(mix_half(c), xm.at[y, :, lanes(c)], misc.at[0])
    own_mix.start()
    for i, (pieces, _, _) in enumerate(weight_slots(c)):
        for src, dst in pieces:
            pltpu.make_async_copy(src, dst, w_local.at[i]).start()

    def weight_whole(i):
        _, src, dst = weight_slots(c)[i]
        return pltpu.make_async_remote_copy(
            src_ref=src,
            dst_ref=dst,
            send_sem=w_send.at[i],
            recv_sem=w_recv.at[i],
            device_id=(ep, partner),
            device_id_type=MESH,
        )

    for copy in small:
        copy.wait()

    tok, top = ex_in.shape[0], routes.shape[0]
    slots_all = n_ep * stride
    rt[...] = jnp.full(rt.shape, -1, jnp.int32)
    rt[0:top, 0:tok] = routes[...]
    tpad[...] = jnp.zeros_like(tpad)
    total_score = scores[0:1, :] + scores[1:2, :]
    tpad[2:3, 0:tok] = scores[0:1, :] / total_score * routed_scale
    tpad[3:4, 0:tok] = scores[1:2, :] / total_score * routed_scale
    xpad[...] = jnp.zeros_like(xpad)
    xpad[0:tok, :] = ex_in[...]
    tokens = rt.shape[1]
    experts = lax.broadcasted_iota(jnp.int32, (n_ep, tokens), 0)
    hit = [experts == rt[k : k + 1, :] for k in range(top)]
    ones = [h.astype(F32) for h in hit]
    before = (
        lax.broadcasted_iota(jnp.int32, (tokens, tokens), 0)
        < lax.broadcasted_iota(jnp.int32, (tokens, tokens), 1)
    ).astype(F32)
    ranks = mm((ones[0] + ones[1]).astype(BF16), before.astype(BF16))
    rows_iota = lax.broadcasted_iota(jnp.int32, (slots_all, tokens), 0)
    table = None
    for k in range(top):
        rank = jnp.sum(ranks * ones[k], axis=0, keepdims=True)
        slot = rt[k : k + 1, :] * stride + rank.astype(jnp.int32)
        tpad[k : k + 1, :] = slot.astype(F32)
        here = rows_iota == slot
        table = here if table is None else table | here
    outgoing = mm(table.astype(F32).astype(BF16), xpad[...]).astype(BF16)
    dsend[...] = outgoing.reshape(dsend.shape)

    pl.semaphore_wait(barrier, 2 * (n_ep - 1) + 3)

    give_mix = pltpu.make_async_remote_copy(
        src_ref=mix_half(o),
        dst_ref=xm.at[y, :, lanes(c)],
        send_sem=misc.at[1],
        recv_sem=misc.at[2],
        device_id=(ep, partner),
        device_id_type=MESH,
    )
    give_mix.start()

    def dispatch_copy(off, e):
        return pltpu.make_async_remote_copy(
            src_ref=dsend.at[e],
            dst_ref=rbuf.at[c, PLACE[off] * n_x + x_own],
            send_sem=s_sem.at[0],
            recv_sem=d_sem.at[PLACE[off]],
            device_id=(e, 2 * y + hs),
            device_id_type=MESH,
        )

    @pl.when(c == hs)
    def _():
        rbuf[c, x_own] = dsend[ep]

    @pl.when(c != hs)
    def _():
        dispatch_copy(0, ep).start()

    for off in sorted(PLACE, key=abs):
        along_x(-off, lambda e: dispatch_copy(off, e).start())

    waiting = [
        (i, src, dst)
        for i, (pieces, _, _) in enumerate(weight_slots(c))
        for src, dst in pieces
    ]

    def feed(count=1):
        for _ in range(min(count, len(waiting))):
            i, src, dst = waiting.pop(0)
            pltpu.make_async_remote_copy(
                src_ref=src,
                dst_ref=dst,
                send_sem=w_send.at[i],
                recv_sem=w_recv.at[i],
                device_id=(ep, partner),
                device_id_type=MESH,
            ).start()

    def gather_block(x, way, part, step):
        rows = x.shape[1] // PARTS
        origin = lax.rem(y + sign[way] * step + n_y, n_y)
        return x.at[origin, pl.ds(part * rows, rows)]

    def gather_copy(x, sem, out, way, part, step):
        block = gather_block(x, way, part, step)
        return pltpu.make_async_remote_copy(
            src_ref=block,
            dst_ref=block,
            send_sem=s_sem.at[out],
            recv_sem=sem.at[place[way, part, step]],
            device_id=(ep, ring_tp[way]),
            device_id_type=MESH,
        )

    def gather_arrived(x, sem, out, way, part, step):
        block = gather_block(x, way, part, step + 1)
        pltpu.make_async_remote_copy(
            src_ref=block,
            dst_ref=block,
            send_sem=s_sem.at[out],
            recv_sem=sem.at[place[way, part, step]],
            device_id=(ep, ring_tp[way]),
            device_id_type=MESH,
        ).wait_recv()

    def gather_start(x, sem, out, parts):
        for part in parts:
            for way in range(2):
                if hops(way, part) > 0:
                    gather_copy(x, sem, out, way, part, 0).start()

    def gather_step(x, sem, out, step, parts=range(PARTS)):
        for way, part in order:
            if part in parts:
                if step < hops(way, part):
                    gather_arrived(x, sem, out, way, part, step)
                    if step + 1 < hops(way, part):
                        gather_copy(x, sem, out, way, part, step + 1).start()
                if way == 1:
                    feed()

    def sent(ref, sem):
        pltpu.make_async_remote_copy(
            src_ref=ref,
            dst_ref=ref,
            send_sem=sem,
            recv_sem=sem,
            device_id=(ep, partner),
            device_id_type=MESH,
        ).wait_send()

    def received(ref, sem):
        pltpu.make_async_remote_copy(
            src_ref=ref,
            dst_ref=ref,
            send_sem=sem,
            recv_sem=sem,
            device_id=(ep, partner),
            device_id_type=MESH,
        ).wait_recv()

    def scale(x, xs, ss, gain, origin):
        cols = pl.ds(pl.multiple_of(origin * W, W), W)
        wide = x[origin].astype(F32)
        square = wide * wide
        ss[...] += square[:, :L] + square[:, L:]
        xs[:, cols] = (wide * gain[:, cols]).astype(BF16)

    def scale_step(x, xs, ss, gain, step):
        scale(x, xs, ss, gain, lax.rem(y + step + 1, n_y))
        if step < long - 1:
            scale(x, xs, ss, gain, lax.rem(y - step - 1 + n_y, n_y))

    def factor_of(ss):
        return lax.rsqrt(jnp.sum(ss[...], axis=1, keepdims=True) / (n_y * W) + epsilon)

    mix = (xm, ag_sem_m, 2)
    exp = (xe, ag_sem_e, 3)
    mix_scale = (xm, xsm, ssm, mix_gain)
    exp_scale = (xe, xse, sse, ex_gain)

    ssm[...] = jnp.zeros_like(ssm)
    sse[...] = jnp.zeros_like(sse)
    own_mix.wait()
    give_mix.wait_recv()
    gather_start(*mix, range(PARTS))
    scale(*mix_scale, y)

    def take_dispatch(part):
        rows, groups = rows_e // PARTS, n_x
        span = pl.ds(part * groups, groups)
        if part == 0:

            @pl.when(c == hs)
            def _():
                received(dsend.at[pl.ds(0, 2 * groups - 1)], d_sem.at[part])

            @pl.when(c != hs)
            def _():
                received(dsend.at[pl.ds(0, 2 * groups)], d_sem.at[part])

        else:
            received(dsend.at[pl.ds(0, 2 * groups)], d_sem.at[part])
        wide = groups * stride
        row = lax.broadcasted_iota(jnp.int32, (rows, wide), 0)
        col = lax.broadcasted_iota(jnp.int32, (rows, wide), 1)
        group = (row * (65536 // cap + 1)) >> 16
        pick = (col - row == group * (stride - cap)).astype(F32).astype(BF16)
        for cs in range(2):
            piece = mm(pick, rbuf[cs, span].reshape(wide, L)).astype(BF16)
            xe[y, part * rows : part * rows + rows, cs * L : cs * L + L] = piece
        gather_start(*exp, (part,))
        if part == PARTS - 1:
            scale(*exp_scale, y)

    def sum_copy(send, recv, sem, out, way, part, step):
        slot = place[way, part, step - (long - hops(way, part))]
        return pltpu.make_async_remote_copy(
            src_ref=send.at[slot],
            dst_ref=recv.at[slot],
            send_sem=s_sem.at[out],
            recv_sem=sem.at[slot],
            device_id=(ep, ring_tp[way]),
            device_id_type=MESH,
        )

    def sum_in(recv, way, part, step):
        return recv[place[way, part, step - (long - hops(way, part))]].astype(F32)

    def prepare(left, right, pre, step):
        half = left.shape[0] // 2
        if step == long:
            cols = pl.ds(pl.multiple_of(y * W, W), W)
            pre[0] = mm(left[...], right[:, cols])
            return
        for way in range(2):
            dest = lax.rem(y - sign[way] * (long - step) + n_y, n_y)
            cols = pl.ds(pl.multiple_of(dest * W, W), W)
            if step < long - short:
                rows = slice(way * half, way * half + half)
                pre[way, rows] = mm(left[rows], right[:, cols])
            else:
                pre[way] = mm(left[...], right[:, cols])

    def sum_step(left, right, pre, send, recv, sem, out, step):
        if step == 0:
            prepare(left, right, pre, 0)
        rows = left.shape[0] // PARTS
        for way, part in last_first:
            first = long - hops(way, part)
            if step < first:
                continue
            value = pre[way, part * rows : part * rows + rows]
            if step > first:
                sum_copy(send, recv, sem, out, way, part, step - 1).wait_recv()
                value = value + sum_in(recv, way, part, step - 1)
            send[place[way, part, step - first]] = value.astype(BF16)
            sum_copy(send, recv, sem, out, way, part, step).start()
        prepare(left, right, pre, step + 1)

    def sum_result(left, right, pre, send, recv, sem, out, part):
        rows = left.shape[0] // PARTS
        value = pre[0, part * rows : part * rows + rows]
        for way in range(2):
            if hops(way, part) > 0:
                sum_copy(send, recv, sem, out, way, part, long - 1).wait_recv()
                value = value + sum_in(recv, way, part, long - 1)
        return value.astype(BF16)

    mix_sum = (gated, wo, pre_m, rs_m_send, rs_m_recv, rs_sem_m, 4)
    exp_sum = (act, wd, pre_e, rs_e_send, rs_e_recv, rs_sem_e, 5)

    def take_weights(lo, hi):
        for i in range(lo, hi):
            _, src, dst = weight_slots(c)[i]
            pltpu.make_async_copy(src, dst, w_local.at[i]).wait()
            weight_whole(i).wait_recv()

    next_ep = jnp.where(c == 0, ep, ep + 1)
    halo = pltpu.make_async_remote_copy(
        src_ref=prod.at[pl.ds(rows_m, 8)],
        dst_ref=prod.at[pl.ds(0, 8)],
        send_sem=misc.at[3],
        recv_sem=misc.at[4],
        device_id=(lax.rem(next_ep, n_ep), partner),
        device_id_type=MESH,
    )
    has_next = jnp.logical_not((c == 1) & (ep == n_ep - 1))
    has_last = jnp.logical_not((c == 0) & (ep == 0))

    def mixer_project():
        factor = factor_of(ssm)
        take_weights(0, 4)
        inner = mm(xsm[...], wm[:, W : 2 * W]) * factor
        values = mm(xsm[...], wm[:, 2 * W :]) * factor
        prod[pl.ds(8, rows_m), :] = inner * values

        @pl.when(has_next)
        def _():
            halo.start()

        outer[...] = mm(xsm[...], wm[:, :W]) * factor

    def mixer_convolve():
        @pl.when(has_last)
        def _():
            halo.wait_recv()

        @pl.when(jnp.logical_not(has_last))
        def _():
            prod[0:8, :] = jnp.zeros((8, W), F32)

        for part in range(2):
            cols = slice(part * L, part * L + L)
            convolved = (
                wc[part, 0:1] * prod[pl.ds(6, rows_m), cols]
                + wc[part, 1:2] * prod[pl.ds(7, rows_m), cols]
                + wc[part, 2:3] * prod[pl.ds(8, rows_m), cols]
            )
            gated[:, cols] = (outer[:, cols] * convolved).astype(BF16)
        take_weights(6, 7)

    def expert_hidden():
        factor = factor_of(sse)
        take_weights(7, 8)
        gate = ga[...] * factor
        up = ua[...] * factor
        act[...] = (gate / (1.0 + jnp.exp(-gate)) * up).astype(BF16)

    def expert_project(step):
        origins = [lax.rem(y + step + 1, n_y)]
        if step < long - 1:
            origins.append(lax.rem(y - step - 1 + n_y, n_y))
        if step == 0:
            origins.append(y)
            take_weights(4, 6)
        for acc, weight in ((ga, wg), (ua, wu)):
            value = None if step == 0 else acc[...]
            for origin in origins:
                cols = pl.ds(pl.multiple_of(origin * W, W), W)
                term = mm_nt(xse[:, cols], weight[:, cols])
                value = term if value is None else value + term
            acc[...] = value

    give_out = pltpu.make_async_remote_copy(
        src_ref=ysend,
        dst_ref=ymo.at[pl.ds(pl.multiple_of(c * rows_m, rows_m), rows_m)],
        send_sem=misc.at[5],
        recv_sem=misc.at[6],
        device_id=(ep, partner),
        device_id_type=MESH,
    )

    def mixer_result():
        half = rows_m // PARTS
        for part in range(PARTS):
            value = sum_result(*mix_sum, part)
            left, right = value[:, :L], value[:, L:]
            mine = jnp.where(c == 0, left, right)
            theirs = jnp.where(c == 0, right, left)
            ymo[pl.ds(pl.multiple_of(c * rows_m + part * half, half), half), :] = mine
            ysend[part * half : part * half + half] = theirs
        give_out.start()

    def return_copy(part, j, cs):
        off = EVEN[part] + odd * (ODD[part] - EVEN[part])
        return pltpu.make_async_remote_copy(
            src_ref=rsend.at[cs, part * n_x + j],
            dst_ref=ret.at[ep],
            send_sem=s_sem.at[6],
            recv_sem=s_sem.at[7],
            device_id=(lax.rem(z + off + Z, Z) * n_x + j, 2 * y + cs),
            device_id_type=MESH,
        )

    def return_part(part):
        value = sum_result(*exp_sum, part)
        groups = n_x
        slots = groups * stride
        row = lax.broadcasted_iota(jnp.int32, (slots, rows_e // PARTS), 0)
        col = lax.broadcasted_iota(jnp.int32, (slots, rows_e // PARTS), 1)
        group = (col * (65536 // cap + 1)) >> 16
        pick = (row - col == group * (stride - cap)).astype(F32).astype(BF16)
        spread = mm(pick, value).astype(BF16)
        for cs in range(2):
            piece = spread[:, cs * L : cs * L + L].reshape(groups, stride, L)
            rsend[cs, part * groups : part * groups + groups] = piece

        def one(i, carry):
            j = lax.rem(x_own + i, n_x)
            for cs in range(2):
                if part == 0:

                    @pl.when(jnp.logical_not((hs == c) & (j == x_own) & (c == cs)))
                    def _():
                        return_copy(part, j, cs).start()

                else:
                    return_copy(part, j, cs).start()
            return carry

        lax.fori_loop(0, groups, one, 0)

    turn = max(1, long - 2)
    gather_step(*mix, 0)
    scale_step(*mix_scale, 0)
    take_dispatch(0)
    if long > 1:
        gather_step(*mix, 1, (0, 1))
        take_dispatch(1)
        gather_step(*mix, 1, (2, 3))
        scale_step(*mix_scale, 1)
    else:
        take_dispatch(1)
    take_dispatch(2)
    if long > 2:
        gather_step(*mix, 2, (0, 1))
        take_dispatch(3)
        gather_step(*mix, 2, (2, 3))
        scale_step(*mix_scale, 2)
    else:
        take_dispatch(3)
    for step in range(3, long):
        for part in range(PARTS):
            gather_step(*exp, step - 3, (part,))
            gather_step(*mix, step, (part,))
        scale_step(*mix_scale, step)
    for step in range(long):
        if step == turn:
            mixer_convolve()
            sum_step(*mix_sum, 0)
        if step >= long - 3 or long < 4:
            gather_step(*exp, step)
        scale_step(*exp_scale, step)
        if step == 0:
            feed(len(waiting))
            mixer_project()
        expert_project(step)
        if step == turn:
            sum_step(*mix_sum, 1)
    if long == 1:
        mixer_convolve()
        sum_step(*mix_sum, 0)
    expert_hidden()
    for step in range(long):
        sum_step(*exp_sum, step)
        if step + 2 < long:
            sum_step(*mix_sum, step + 2)
    mixer_result()
    for part in reversed(range(PARTS)):
        return_part(part)

    @pl.when(c == hs)
    def _():
        ret[ep] = rsend[c, x_own]

    give_out.wait_recv()
    mix_out[...] = ymo[...]

    tcol = jnp.transpose(tpad[...])
    lane = lax.broadcasted_iota(jnp.int32, (tok, slots_all), 1)

    picks = [
        (lane == tcol[0:tok, k : k + 1].astype(jnp.int32)).astype(F32).astype(BF16)
        for k in range(top)
    ]

    @pl.when(c == hs)
    def _():
        sent(dsend.at[pl.ds(0, n_ep - 1)], s_sem.at[0])
        sent(dsend.at[pl.ds(0, n_ep - 1)], s_sem.at[6])

    @pl.when(c != hs)
    def _():
        sent(dsend, s_sem.at[0])
        sent(dsend, s_sem.at[6])

    give_mix.wait_send()
    for i in range(8):
        weight_whole(i).wait_send()

    @pl.when(has_next)
    def _():
        halo.wait_send()

    give_out.wait_send()
    sent(xm.at[pl.ds(0, n_y - 1)], s_sem.at[2])
    sent(xe.at[pl.ds(0, n_y - 1)], s_sem.at[3])
    sent(rs_m_send, s_sem.at[4])
    sent(rs_e_send, s_sem.at[5])

    @pl.when(c == hs)
    def _():
        received(dsend.at[pl.ds(0, n_ep - 1)], s_sem.at[7])

    @pl.when(c != hs)
    def _():
        received(dsend, s_sem.at[7])

    back = ret[...].reshape(slots_all, L)
    total = None
    for k in range(top):
        term = mm(picks[k], back) * tcol[0:tok, 2 + k : 3 + k]
        total = term if total is None else total + term
    ex_out[...] = total.astype(BF16)


def local(
    mix_input,
    mix_gain,
    gate_b_weight,
    gate_c_weight,
    value_weight,
    conv_weight,
    out_weight,
    expert_input,
    expert_gain,
    routes,
    route_weight,
    expert_gate,
    expert_up,
    expert_down,
):
    n_ep, n_tp = lax.axis_size("ep"), lax.axis_size("tp")
    n_y = n_tp // 2
    tok, top = routes.shape
    cap = 2 * tok * top // n_ep
    stride = -(-cap // 8) * 8
    half_ep = n_ep // 2
    rows_m = mix_input.shape[0] // 2
    rows_e = half_ep * cap
    width = mix_gain.shape[0]
    hid = expert_gate.shape[2]
    tokens = -(-tok // L) * L
    long = n_y // 2
    slots_all = n_ep * stride
    dma = pltpu.SemaphoreType.DMA
    any_spec = pl.BlockSpec(memory_space=pl.ANY)
    vmem = pl.BlockSpec(memory_space=pltpu.VMEM)
    scratch = [
        pltpu.VMEM((1, width), F32),
        pltpu.VMEM((1, width), F32),
        pltpu.VMEM((top, tok), jnp.int32),
        pltpu.VMEM((top, tok), F32),
        pltpu.VMEM((tok, L), BF16),
        pltpu.VMEM((rows_e, 2 * hid), F32),
        pltpu.VMEM((rows_e, 2 * hid), F32),
        pltpu.VMEM((n_y, rows_m, W), BF16),
        pltpu.VMEM((n_y, rows_e, W), BF16),
        pltpu.VMEM((rows_m, width), BF16),
        pltpu.VMEM((rows_e, width), BF16),
        pltpu.VMEM((rows_m, L), F32),
        pltpu.VMEM((rows_e, L), F32),
        pltpu.VMEM((width, 3 * W), BF16),
        pltpu.VMEM((W, width), BF16),
        pltpu.VMEM((2 * hid, width), BF16),
        pltpu.VMEM((2 * hid, width), BF16),
        pltpu.VMEM((2 * hid, width), BF16),
        pltpu.VMEM((2, 3, L), F32),
        pltpu.VMEM((8, tokens), jnp.int32),
        pltpu.VMEM((8, tokens), F32),
        pltpu.VMEM((tokens, L), BF16),
        pltpu.VMEM((n_ep, stride, L), BF16),
        pltpu.VMEM((2, half_ep, stride, L), BF16),
        pltpu.VMEM((8 + rows_m, W), F32),
        pltpu.VMEM((rows_m, W), F32),
        pltpu.VMEM((rows_m, W), BF16),
        pltpu.VMEM((rows_e, 2 * hid), BF16),
        pltpu.VMEM((PARTS * (n_y - 1), rows_m // PARTS, W), BF16),
        pltpu.VMEM((PARTS * (n_y - 1), rows_m // PARTS, W), BF16),
        pltpu.VMEM((PARTS * (n_y - 1), rows_e // PARTS, W), BF16),
        pltpu.VMEM((PARTS * (n_y - 1), rows_e // PARTS, W), BF16),
        pltpu.VMEM((2 * rows_m, L), BF16),
        pltpu.VMEM((rows_m, L), BF16),
        pltpu.VMEM((2, half_ep, stride, L), BF16),
        pltpu.VMEM((n_ep, stride, L), BF16),
        pltpu.VMEM((2, rows_m, W), F32),
        pltpu.VMEM((2, rows_e, W), F32),
        dma((PARTS * (n_y - 1),)),
        dma((PARTS * (n_y - 1),)),
        dma((PARTS * (n_y - 1),)),
        dma((PARTS * (n_y - 1),)),
        dma((8,)),
        dma((PARTS,)),
        dma((8,)),
        dma((8,)),
        dma((8,)),
        dma((5,)),
        dma((7,)),
    ]
    return pl.pallas_call(
        functools.partial(kernel, n_ep, n_y, cap, stride),
        out_shape=(
            pltpu.VMEM(mix_input.shape, BF16),
            pltpu.VMEM(expert_input.shape, BF16),
        ),
        in_specs=[any_spec] * 14,
        out_specs=(vmem, vmem),
        scratch_shapes=scratch,
        compiler_params=pltpu.CompilerParams(
            collective_id=0, has_side_effects=True, vmem_limit_bytes=56 * 1024 * 1024
        ),
    )(
        mix_input,
        mix_gain.reshape(1, width),
        gate_b_weight,
        gate_c_weight,
        value_weight,
        conv_weight,
        out_weight,
        expert_input,
        expert_gain.reshape(1, width),
        routes.T,
        route_weight.T,
        jnp.swapaxes(expert_gate, 1, 2)[0],
        jnp.swapaxes(expert_up, 1, 2)[0],
        expert_down[0],
    )


def solution(mesh):
    in_specs = (
        P("ep", "tp"),
        P(),
        P(None, "tp"),
        P(None, "tp"),
        P(None, "tp"),
        P(None, "tp"),
        P("tp", None),
        P("ep", "tp"),
        P(),
        P("ep", None),
        P("ep", None),
        P("ep", None, "tp"),
        P("ep", None, "tp"),
        P("ep", "tp", None),
    )
    out_specs = (P("ep", "tp"), P("ep", "tp"))
    return jax.shard_map(local, mesh=mesh, in_specs=in_specs, out_specs=out_specs, check_vma=False)
```

time: 85.1 us -> 73.7 us (0.87)
  Pallas kernels: 82.1 us -> 71.7 us
  local copies, waits for them, and re-layouts: 2.17 us -> 1.26 us
    pallas_call x1, Pallas kernels: 82.1 us -> 71.7 us  [local(): pl.pallas_call(functools.partial(kernel, n_ep, n_y, cap, stride), out_sha...]
    unnamed x4 -> x2, local copies, waits for them, and re-layouts: 2.17 us -> 1.26 us
where the time goes in v2:
time: 73.7 us; the launch traced here: 73.6 us
  Pallas kernels  71.7 us (97%)
  local copies, waits for them, and re-layouts  1.26 us (2%)
    pallas_call x1, Pallas kernels, local(): pl.pallas_call(functools.partial(kernel, n_ep, n_y, cap, stride), out_sha...  71.7 us

profile of v2, /device:TPU:1, one launch (start us, length us, event | category | flops | bytes accessed | tf_op | source)
XLA Modules:
  0.0 73.6 jit_solution(13592970368278550995)
XLA Ops:
  0.6 71.7 %shard_map.149 = (bf16[384,128]{1,0:T(8,128)(2,1)S(1)}, bf16[160,128]{1,0:T(8,128)(2,1)S(1)}) custom-call(bf16[384,128]{1,0:T(8,128)(2,1)} %mix_in.1, f32[1,2048]{1,0:T(1,128)} %bitcast.14, bf16[2048,128]{1,0:T(8,128)(2,1)} %gb.1, bf16[2048,128]{1,0:T(8,128)(2,1)} %gc.1, bf16[2048,128]{1,0:T(8,128)(2,1)} %vw.1, f32[3,128]{1,0:T(4,128)} %cw.1, ...), custom_call_target="tpu_custom_call" | custom-call | tf_op jit(solution)/shard_map/pallas_call | solution.py:793
  72.3 0.6 copy.18
  72.9 0.6 copy.19

commit v3 on v0

v3 whole, which is shorter than its diff:
```python
import functools

import jax
import jax.numpy as jnp
from jax import lax
from jax.experimental import pallas as pl
from jax.experimental.pallas import tpu as pltpu
from jax.sharding import PartitionSpec as P

epsilon = 1e-06
routed_scale = 2.5
MESH = pl.DeviceIdType.MESH
F32 = jnp.float32
BF16 = jnp.bfloat16
L = 128
W = 2 * L
MIX_PARTS = 4
Z = 8
OFFS = (0, 1, -1, 2, -2, 3, -3, 4)


def mm(a, b):
    return jnp.dot(a, b, preferred_element_type=F32)


def mm_nt(a, b):
    return lax.dot_general(a, b, (((1,), (1,)), ((), ())), preferred_element_type=F32)


def kernel(*args):
    for core in range(2):

        @pl.when(lax.rem(lax.axis_index("tp"), 2) == core)
        def _():
            body(core, *args)


def body(
    c,
    n_ep,
    n_y,
    cap,
    stride,
    mix_in,
    mix_gain_in,
    gb,
    gc,
    vw,
    cw,
    ow,
    ex_in_in,
    ex_gain_in,
    routes_in,
    scores_in,
    eg,
    eu,
    ed,
    out,
    gain,
    routes,
    scores,
    ex_in,
    acc_gate,
    acc_up,
    xm,
    xe,
    xsm,
    xse,
    ssm,
    sse,
    wm,
    wo,
    wg,
    wu,
    wd,
    wc,
    rt,
    tpad,
    xpad,
    dsend,
    rbuf,
    prod,
    outer,
    gated,
    act,
    rs_m_send,
    rs_m_recv,
    rs_e_send,
    rs_e_recv,
    ymo,
    rsend,
    ret,
    pre_m,
    pre_e,
    ag_sem,
    rs_sem,
    s_sem,
    d_sem,
    w_local,
    w_send,
    w_recv,
    i_sem,
    misc,
    go,
    acc_mix,
):
    ep = lax.axis_index("ep")
    tp = lax.axis_index("tp")
    y = tp // 2
    partner = 2 * y + 1 - c
    n_x = n_ep // Z
    z, x_own = ep // n_x, lax.rem(ep, n_x)
    long, short = n_y // 2, n_y - 1 - n_y // 2
    ring_tp = (2 * lax.rem(y + n_y - 1, n_y) + c, 2 * lax.rem(y + 1, n_y) + c)
    sign = (1, -1)
    hid = wg.shape[0] // 2
    tok, top = ex_in.shape[0], routes.shape[0]
    rows_m = xm.shape[1]
    x, xs, ss = ((xm, xsm, ssm), (xe, xse, sse))[c]
    send, recv, pre = ((rs_m_send, rs_m_recv, pre_m), (rs_e_send, rs_e_recv, pre_e))[c]
    parts = (MIX_PARTS, Z)[c]
    rows = x.shape[1] // parts

    def hops(way, part):
        return long if way == part % 2 else short

    order = [(way, part) for part in range(parts) for way in range(2)]
    last_first = [(way, part) for part in reversed(range(parts)) for way in range(2)]
    place = {}
    for step in range(long):
        for way, part in order:
            if step < hops(way, part):
                place[way, part, step] = len(place)

    def remote(src, dst, send_sem, recv_sem, device):
        return pltpu.make_async_remote_copy(
            src_ref=src,
            dst_ref=dst,
            send_sem=send_sem,
            recv_sem=recv_sem,
            device_id=device,
            device_id_type=MESH,
        )

    def sent(ref, sem):
        remote(ref, ref, sem, sem, (ep, partner)).wait_send()

    def received(ref, sem):
        remote(ref, ref, sem, sem, (ep, partner)).wait_recv()

    barrier = pltpu.get_barrier_semaphore()

    def along_x(off, act_on):
        def one(j, carry):
            act_on(lax.rem(z + off + Z, Z) * n_x + lax.rem(x_own + j, n_x))
            return carry

        lax.fori_loop(1 if off == 0 else 0, n_x, one, 0)

    small = [
        pltpu.make_async_copy(src, dst, i_sem.at[i])
        for i, (src, dst) in enumerate(
            (
                (routes_in, routes),
                (scores_in, scores),
                (ex_in_in, ex_in),
                ((mix_gain_in, ex_gain_in)[c], gain),
            )
        )
    ]
    for copy in small:
        copy.start()

    def greet(e):
        pl.semaphore_signal(barrier, inc=1, device_id=(e, 2 * y), device_id_type=MESH)
        pl.semaphore_signal(barrier, inc=1, device_id=(e, 2 * y + 1), device_id_type=MESH)

    for off in reversed(OFFS):
        along_x(off, greet)
    for t in ring_tp + (partner,):
        pl.semaphore_signal(barrier, inc=1, device_id=(ep, t), device_id_type=MESH)

    def weight_slots(core, who):
        if core == 0:
            return (
                (gb, wm.at[:, pl.ds(who * L, L)]),
                (gc, wm.at[:, pl.ds(W + who * L, L)]),
                (vw, wm.at[:, pl.ds(2 * W + who * L, L)]),
                (cw, wc.at[who]),
                (ow, wo.at[pl.ds(who * L, L)]),
            )
        return (
            (eg, wg.at[pl.ds(who * hid, hid)]),
            (eu, wu.at[pl.ds(who * hid, hid)]),
            (ed, wd.at[pl.ds(who * hid, hid)]),
        )

    own_weights = [
        pltpu.make_async_copy(src, dst, w_local.at[i])
        for i, (src, dst) in enumerate(weight_slots(c, c))
    ]
    give_weights = [
        remote(src, dst, w_send.at[i], w_recv.at[i], (ep, partner))
        for i, (src, dst) in enumerate(weight_slots(1 - c, c))
    ]
    if c == 0:
        own_mix = pltpu.make_async_copy(mix_in, xm.at[y, :, pl.ds(0, L)], misc.at[0])
        own_mix.start()
    for copy in own_weights:
        copy.start()

    def take_weights(lo, hi):
        for i in range(lo, hi):
            own_weights[i].wait()
            received(weight_slots(c, 1 - c)[i][1], w_recv.at[i])

    for copy in small:
        copy.wait()

    slots_all = n_ep * stride
    rt[...] = jnp.full(rt.shape, -1, jnp.int32)
    rt[0:top, 0:tok] = routes[...]
    tpad[...] = jnp.zeros_like(tpad)
    total_score = scores[0:1, :] + scores[1:2, :]
    tpad[2:3, 0:tok] = scores[0:1, :] / total_score * routed_scale
    tpad[3:4, 0:tok] = scores[1:2, :] / total_score * routed_scale
    xpad[...] = jnp.zeros_like(xpad)
    xpad[0:tok, :] = ex_in[...]
    tokens = rt.shape[1]
    experts = lax.broadcasted_iota(jnp.int32, (n_ep, tokens), 0)
    ones = [(experts == rt[k : k + 1, :]).astype(F32) for k in range(top)]
    before = (
        lax.broadcasted_iota(jnp.int32, (tokens, tokens), 0)
        < lax.broadcasted_iota(jnp.int32, (tokens, tokens), 1)
    ).astype(F32)
    ranks = mm((ones[0] + ones[1]).astype(BF16), before.astype(BF16))
    rows_iota = lax.broadcasted_iota(jnp.int32, (slots_all, tokens), 0)
    table = None
    for k in range(top):
        rank = jnp.sum(ranks * ones[k], axis=0, keepdims=True)
        slot = rt[k : k + 1, :] * stride + rank.astype(jnp.int32)
        tpad[k : k + 1, :] = slot.astype(F32)
        here = rows_iota == slot
        table = here if table is None else table | here
    outgoing = mm(table.astype(F32).astype(BF16), xpad[...]).astype(BF16)
    dsend[...] = outgoing.reshape(dsend.shape)
    ss[...] = jnp.zeros_like(ss)

    pl.semaphore_wait(barrier, 2 * (n_ep - 1) + 3)

    if c == 1:
        give_mix = remote(
            mix_in, xm.at[y, :, pl.ds(L, L)], misc.at[1], misc.at[2], (ep, partner)
        )
        give_mix.start()

    def dispatch_copy(index, e):
        return remote(
            dsend.at[e],
            rbuf.at[c, index * n_x + x_own],
            s_sem.at[0],
            d_sem.at[index],
            (e, 2 * y + 1),
        )

    if c == 1:
        rbuf[1, x_own] = dsend[ep]
    else:
        dispatch_copy(0, ep).start()
    for index, off in enumerate(OFFS):
        along_x(-off, lambda e: dispatch_copy(index, e).start())
    for copy in give_weights:
        copy.start()

    def gather_block(way, part, step):
        origin = lax.rem(y + sign[way] * step + n_y, n_y)
        return x.at[origin, pl.ds(part * rows, rows)]

    def gather_send(way, part, step):
        block = gather_block(way, part, step)
        sem = ag_sem.at[place[way, part, step]]
        remote(block, block, s_sem.at[1], sem, (ep, ring_tp[way])).start()

    def gather_start(part):
        for way in range(2):
            if hops(way, part) > 0:
                gather_send(way, part, 0)

    def gather_step(step, some):
        for way, part in order:
            if part in some and step < hops(way, part):
                received(gather_block(way, part, step + 1), ag_sem.at[place[way, part, step]])
                if step + 1 < hops(way, part):
                    gather_send(way, part, step + 1)

    def scale(origin):
        cols = pl.ds(pl.multiple_of(origin * W, W), W)
        wide = x[origin].astype(F32)
        square = wide * wide
        ss[...] += square[:, :L] + square[:, L:]
        xs[:, cols] = (wide * gain[:, cols]).astype(BF16)

    def origins_of(step):
        found = [lax.rem(y + step + 1, n_y)]
        if step < long - 1:
            found.append(lax.rem(y - step - 1 + n_y, n_y))
        return found

    def scale_step(step):
        for origin in origins_of(step):
            scale(origin)

    def factor_of(lo=0, hi=x.shape[1]):
        return lax.rsqrt(jnp.sum(ss[lo:hi], axis=1, keepdims=True) / (n_y * W) + epsilon)

    left, right = ((gated, wo), (act, wd))[c]

    def sum_slot(way, part, step):
        return place[way, part, step - (long - hops(way, part))]

    def sum_in(way, part, step):
        slot = sum_slot(way, part, step)
        received(recv.at[slot], rs_sem.at[slot])
        return recv[slot].astype(F32)

    def prepare(step, lo=0, hi=x.shape[1]):
        for way in range(2 if 0 < step < long else 1):
            dest = y if step == long else lax.rem(y - sign[way] * (long - step) + n_y, n_y)
            cols = pl.ds(pl.multiple_of(dest * W, W), W)
            pre[way, lo:hi] = mm(left[lo:hi], right[:, cols])

    def sum_sends(step, some):
        for way, part in last_first:
            first = long - hops(way, part)
            if step < first or part not in some:
                continue
            value = pre[way if step > 0 else 0, part * rows : part * rows + rows]
            if step > first:
                value = value + sum_in(way, part, step - 1)
            slot = sum_slot(way, part, step)
            send[slot] = value.astype(BF16)
            remote(
                send.at[slot], recv.at[slot], s_sem.at[2], rs_sem.at[slot], (ep, ring_tp[way])
            ).start()

    def sum_step(step):
        sum_sends(step, range(parts))
        prepare(step + 1)

    def sum_result(part):
        value = pre[0, part * rows : part * rows + rows]
        for way in range(2):
            if hops(way, part) > 0:
                value = value + sum_in(way, part, long - 1)
        return value.astype(BF16)

    def slot_table(shape, row_dim):
        row = lax.broadcasted_iota(jnp.int32, shape, row_dim)
        slot = lax.broadcasted_iota(jnp.int32, shape, 1 - row_dim)
        group = (row * (65536 // cap + 1)) >> 16
        return (slot - row == group * (stride - cap)).astype(F32).astype(BF16)

    if c == 0:
        own_mix.wait()
        received(xm.at[y, :, pl.ds(L, L)], misc.at[2])
        for part in range(parts):
            gather_start(part)
        scale(y)
        for step in range(long):
            gather_step(step, range(parts))
            scale_step(step)
            origins = origins_of(step)
            if step == 0:
                origins.append(y)
                take_weights(0, 4)
            value = None if step == 0 else acc_mix[...]
            for origin in origins:
                cols = pl.ds(pl.multiple_of(origin * W, W), W)
                term = mm(xs[:, cols], wm[cols, :])
                value = term if value is None else value + term
            acc_mix[...] = value

        factor = factor_of()

        def product(lo, hi):
            part = factor[lo:hi]
            inner = acc_mix[lo:hi, W : 2 * W] * part
            prod[8 + lo : 8 + hi, :] = inner * (acc_mix[lo:hi, 2 * W :] * part)

        product(rows_m - 16, rows_m)
        halo = remote(
            prod.at[pl.ds(rows_m, 8)],
            prod.at[pl.ds(0, 8)],
            misc.at[3],
            misc.at[4],
            (lax.rem(ep + 1, n_ep), tp),
        )

        @pl.when(ep < n_ep - 1)
        def _():
            halo.start()

        product(0, rows_m - 16)
        outer[...] = acc_mix[:, :W] * factor

        take_weights(4, 5)

        def convolve(lo, hi):
            for h in range(2):
                cols = slice(h * L, h * L + L)
                convolved = (
                    wc[h, 0:1] * prod[6 + lo : 6 + hi, cols]
                    + wc[h, 1:2] * prod[7 + lo : 7 + hi, cols]
                    + wc[h, 2:3] * prod[8 + lo : 8 + hi, cols]
                )
                gated[lo:hi, cols] = (outer[lo:hi, cols] * convolved).astype(BF16)

        convolve(16, rows_m)
        prepare(0, rows, rows_m)
        sum_sends(0, range(1, parts))

        @pl.when(ep > 0)
        def _():
            halo.wait_recv()

        @pl.when(ep == 0)
        def _():
            prod[0:8, :] = jnp.zeros((8, W), F32)

        convolve(0, 16)
        prepare(0, 0, rows)
        sum_sends(0, (0,))
        prepare(1)
        for step in range(1, long):
            if step == long - 1:
                pl.semaphore_wait(go.at[0], 1)
            sum_step(step)
        if long == 1:
            pl.semaphore_wait(go.at[0], 1)
        give_out = remote(ymo, ymo, misc.at[5], misc.at[6], (ep, partner))
        for part in range(parts):
            value = sum_result(part)
            out[part * rows : part * rows + rows, :] = value[:, :L]
            ymo[part * rows : part * rows + rows, :] = value[:, L:]
        give_out.start()
    else:

        def take_dispatch(part):
            count = 2 * n_x - (1 if part == 0 else 0)
            received(dsend.at[pl.ds(0, count)], d_sem.at[part])
            pick = slot_table((rows, n_x * stride), 0)
            for cs in range(2):
                block = rbuf[cs, pl.ds(part * n_x, n_x)].reshape(n_x * stride, L)
                piece = mm(pick, block).astype(BF16)
                xe[y, part * rows : part * rows + rows, cs * L : cs * L + L] = piece
            gather_start(part)

        def project(step):
            origins = origins_of(step)
            if step == 0:
                origins.append(y)
                take_weights(0, 2)
            for acc, weight in ((acc_gate, wg), (acc_up, wu)):
                value = None if step == 0 else acc[...]
                for origin in origins:
                    cols = pl.ds(pl.multiple_of(origin * W, W), W)
                    term = mm_nt(xs[:, cols], weight[:, cols])
                    value = term if value is None else value + term
                acc[...] = value

        for part in range(parts):
            take_dispatch(part)
            if part >= parts // 2 - 1:
                gather_step(0, (part - parts // 2 + 1,))
        scale(y)
        gather_step(0, range(parts // 2 + 1, parts))
        if long > 1:
            gather_step(1, range(parts))
        scale_step(0)
        project(0)
        for step in range(1, long):
            if step > 1:
                gather_step(step, range(parts))
            scale_step(step)
            project(step)
        take_weights(2, 3)
        half = x.shape[1] // 2
        for lo in (half, 0):
            factor = factor_of(lo, lo + half)
            gate = acc_gate[lo : lo + half] * factor
            up = acc_up[lo : lo + half] * factor
            act[lo : lo + half] = (gate / (1.0 + jnp.exp(-gate)) * up).astype(BF16)
            prepare(0, lo, lo + half)
            sum_sends(0, range(lo // rows, (lo + half) // rows))
        prepare(1)
        for step in range(1, long):
            sum_step(step)

        def return_copy(part, j, cs):
            return remote(
                rsend.at[cs, part * n_x + j],
                ret.at[ep],
                s_sem.at[3 + cs],
                s_sem.at[5],
                (lax.rem(z + OFFS[part] + Z, Z) * n_x + j, 2 * y + cs),
            )

        spread_table = slot_table((n_x * stride, rows), 1)
        for part in reversed(range(parts)):
            spread = mm(spread_table, sum_result(part)).astype(BF16)
            if part == 4:
                pl.semaphore_signal(
                    go.at[0], inc=1, device_id=(ep, partner), device_id_type=MESH
                )
            for cs in range(2):
                piece = spread[:, cs * L : cs * L + L].reshape(n_x, stride, L)
                rsend[cs, part * n_x : part * n_x + n_x] = piece

            def one(i, carry):
                j = lax.rem(x_own + i, n_x)
                return_copy(part, j, 0).start()
                if part > 0:
                    return_copy(part, j, 1).start()
                else:

                    @pl.when(j != x_own)
                    def _():
                        return_copy(part, j, 1).start()

                return carry

            lax.fori_loop(0, n_x, one, 0)
        ret[ep] = rsend[1, x_own]

    tcol = jnp.transpose(tpad[...])
    lane = lax.broadcasted_iota(jnp.int32, (tok, slots_all), 1)
    picks = [
        (lane == tcol[0:tok, k : k + 1].astype(jnp.int32)).astype(F32).astype(BF16)
        for k in range(top)
    ]
    for i in range(len(give_weights)):
        give_weights[i].wait_send()
    sent(dsend.at[pl.ds(0, n_ep - c)], s_sem.at[0])
    sent(x.at[pl.ds(0, n_y - 1)], s_sem.at[1])
    sent(send, s_sem.at[2])
    if c == 0:

        @pl.when(ep < n_ep - 1)
        def _():
            halo.wait_send()

        give_out.wait_send()
    else:
        give_mix.wait_send()
        received(ymo, misc.at[6])
        out[pl.ds(0, rows_m), :] = ymo[...]
        sent(rsend.at[0], s_sem.at[3])
        sent(rsend.at[1, pl.ds(0, n_ep - 1)], s_sem.at[4])
    received(dsend.at[pl.ds(0, n_ep - c)], s_sem.at[5])
    back = ret[...].reshape(slots_all, L)
    total = None
    for k in range(top):
        term = mm(picks[k], back) * tcol[0:tok, 2 + k : 3 + k]
        total = term if total is None else total + term
    out[pl.ds(rows_m, tok), :] = total.astype(BF16)


def local(
    mix_input,
    mix_gain,
    gate_b_weight,
    gate_c_weight,
    value_weight,
    conv_weight,
    out_weight,
    expert_input,
    expert_gain,
    routes,
    route_weight,
    expert_gate,
    expert_up,
    expert_down,
):
    n_ep, n_tp = lax.axis_size("ep"), lax.axis_size("tp")
    n_y = n_tp // 2
    tok, top = routes.shape
    cap = 2 * tok * top // n_ep
    stride = -(-cap // 8) * 8
    rows_m = mix_input.shape[0]
    rows_e = n_ep * cap
    width = mix_gain.shape[0]
    hid = expert_gate.shape[2]
    tokens = -(-tok // L) * L
    mix_slots, ex_slots = MIX_PARTS * (n_y - 1), Z * (n_y - 1)
    dma = pltpu.SemaphoreType.DMA
    any_spec = pl.BlockSpec(memory_space=pl.ANY)
    vmem = pl.BlockSpec(memory_space=pltpu.VMEM)
    scratch = [
        pltpu.VMEM((1, width), F32),
        pltpu.VMEM((top, tok), jnp.int32),
        pltpu.VMEM((top, tok), F32),
        pltpu.VMEM((tok, L), BF16),
        pltpu.VMEM((rows_e, 2 * hid), F32),
        pltpu.VMEM((rows_e, 2 * hid), F32),
        pltpu.VMEM((n_y, rows_m, W), BF16),
        pltpu.VMEM((n_y, rows_e, W), BF16),
        pltpu.VMEM((rows_m, width), BF16),
        pltpu.VMEM((rows_e, width), BF16),
        pltpu.VMEM((rows_m, L), F32),
        pltpu.VMEM((rows_e, L), F32),
        pltpu.VMEM((width, 3 * W), BF16),
        pltpu.VMEM((W, width), BF16),
        pltpu.VMEM((2 * hid, width), BF16),
        pltpu.VMEM((2 * hid, width), BF16),
        pltpu.VMEM((2 * hid, width), BF16),
        pltpu.VMEM((2, 3, L), F32),
        pltpu.VMEM((8, tokens), jnp.int32),
        pltpu.VMEM((8, tokens), F32),
        pltpu.VMEM((tokens, L), BF16),
        pltpu.VMEM((n_ep, stride, L), BF16),
        pltpu.VMEM((2, n_ep, stride, L), BF16),
        pltpu.VMEM((8 + rows_m, W), F32),
        pltpu.VMEM((rows_m, W), F32),
        pltpu.VMEM((rows_m, W), BF16),
        pltpu.VMEM((rows_e, 2 * hid), BF16),
        pltpu.VMEM((mix_slots, rows_m // MIX_PARTS, W), BF16),
        pltpu.VMEM((mix_slots, rows_m // MIX_PARTS, W), BF16),
        pltpu.VMEM((ex_slots, rows_e // Z, W), BF16),
        pltpu.VMEM((ex_slots, rows_e // Z, W), BF16),
        pltpu.VMEM((rows_m, L), BF16),
        pltpu.VMEM((2, n_ep, stride, L), BF16),
        pltpu.VMEM((n_ep, stride, L), BF16),
        pltpu.VMEM((2, rows_m, W), F32),
        pltpu.VMEM((2, rows_e, W), F32),
        dma((ex_slots,)),
        dma((ex_slots,)),
        dma((6,)),
        dma((Z,)),
        dma((5,)),
        dma((5,)),
        dma((5,)),
        dma((4,)),
        dma((7,)),
        pltpu.SemaphoreType.REGULAR((1,)),
        pltpu.VMEM((rows_m, 3 * W), F32),
    ]
    both = pl.pallas_call(
        functools.partial(kernel, n_ep, n_y, cap, stride),
        out_shape=pltpu.VMEM((mix_input.shape[0] + tok, L), BF16),
        in_specs=[any_spec] * 14,
        out_specs=vmem,
        scratch_shapes=scratch,
        compiler_params=pltpu.CompilerParams(
            collective_id=0, has_side_effects=True, vmem_limit_bytes=56 * 1024 * 1024
        ),
    )(
        mix_input,
        mix_gain.reshape(1, width),
        gate_b_weight,
        gate_c_weight,
        value_weight,
        conv_weight,
        out_weight,
        expert_input,
        expert_gain.reshape(1, width),
        routes.T,
        route_weight.T,
        jnp.swapaxes(expert_gate, 1, 2)[0],
        jnp.swapaxes(expert_up, 1, 2)[0],
        expert_down[0],
    )
    return both[: mix_input.shape[0]], both[mix_input.shape[0] :]


def solution(mesh):
    in_specs = (
        P("ep", "tp"),
        P(),
        P(None, "tp"),
        P(None, "tp"),
        P(None, "tp"),
        P(None, "tp"),
        P("tp", None),
        P("ep", "tp"),
        P(),
        P("ep", None),
        P("ep", None),
        P("ep", None, "tp"),
        P("ep", None, "tp"),
        P("ep", "tp", None),
    )
    out_specs = (P("ep", "tp"), P("ep", "tp"))
    return jax.shard_map(local, mesh=mesh, in_specs=in_specs, out_specs=out_specs, check_vma=False)
```

time: 210 us -> 68.6 us (0.33); the launches traced: 207 us -> 68.4 us
  waiting for transfers between devices: 120 us -> 0 us
  Pallas kernels: 0 us -> 66.5 us
  blocking collectives: 23.6 us -> 0 us
  between operations: 14.3 us -> 0.64 us
  matrix products: 13.5 us -> 0 us
  local copies, waits for them, and re-layouts: 13.8 us -> 1.27 us
  starting transfers between devices: 11.3 us -> 0 us
  other arithmetic: 11 us -> 0 us
    pallas_call x0 -> x1, Pallas kernels: none -> 66.5 us  [local(): pl.pallas_call(functools.partial(kernel, n_ep, n_y, cap, stride), out_sha...]
    unnamed x3 -> x0, waiting for transfers between devices: 62.4 us -> none
    all_gather x1 -> x0, waiting for transfers between devices: 49.4 us -> none  [side_by_side(): out, at, done = (lax.all_gather(both, axis, axis=dim, tiled=True), 0, [])]
    all_to_all x1 -> x0, blocking collectives: 23.6 us -> none  [local(): lax.all_to_all(outgoing, 'ep', split_axis=0, concat_axis=2, tiled=True)]
    dot_general x7 -> x0, matrix products: 13.5 us -> none  [the longest x1 4.83 us: local(): lax.dot_general(out_weight, gated, (((0,), (1,)), ((), ())), preferred_el...]
    all_to_all x1 -> x0, starting transfers between devices: 9.08 us -> none  [local(): lax.all_to_all(returning, 'ep', split_axis=2, concat_axis=2, tiled=True)]
    unnamed x22 -> x0, local copies, waits for them, and re-layouts: 8.89 us -> none
    all_to_all x1 -> x0, waiting for transfers between devices: 7.75 us -> none  [local(): lax.all_to_all(returning, 'ep', split_axis=2, concat_axis=2, tiled=True)]
  transfers between devices with their start and end apart: 4 -> 0, of which waited for: 3 -> 0; matrix products, arithmetic and copies ran while one was open for 4% -> 0% of each run, Pallas kernels for 0% -> 0%
where the time goes in v3:
time: 68.6 us; the launch traced here: 68.4 us
  Pallas kernels  66.5 us (97%)
  local copies, waits for them, and re-layouts  1.27 us (2%)
    pallas_call x1, Pallas kernels, local(): pl.pallas_call(functools.partial(kernel, n_ep, n_y, cap, stride), out_sha...  66.5 us

profile of v3, /device:TPU:1, one launch (start us, length us, event | category | flops | bytes accessed | tf_op | source)
XLA Modules:
  0.0 68.4 jit_solution(11252406999494887715)
XLA Ops:
  0.6 66.5 %shard_map.149 = bf16[544,128]{1,0:T(8,128)(2,1)S(1)} custom-call(bf16[384,128]{1,0:T(8,128)(2,1)} %args_0_.4, f32[1,2048]{1,0:T(1,128)} %bitcast.14, bf16[2048,128]{1,0:T(8,128)(2,1)} %args_2_.4, bf16[2048,128]{1,0:T(8,128)(2,1)} %args_3_.4, bf16[2048,128]{1,0:T(8,128)(2,1)} %args_4_.4, f32[3,128]{1,0:T(4,128)} %args_5_.4, bf16[128,2048]{1,0:T(8,128)(2,1)} %args_6_.4, ...), custom_call_target="tpu_custom_call" | custom-call | tf_op jit(solution)/shard_map/pallas_call | solution.py:647
  67.1 0.6 slice.7
  67.7 0.6 slice.6

commit v4 on v3

--- a/solution.py
+++ b/solution.py
@@ -88,6 +88,8 @@
     rs_e_send,
     rs_e_recv,
     ymo,
+    ysend,
+    yrecv,
     rsend,
     ret,
     pre_m,
@@ -177,7 +179,8 @@
 
     for off in reversed(OFFS):
         along_x(off, greet)
-    for t in ring_tp + (partner,):
+    other_tp = tuple(t + 1 - 2 * c for t in ring_tp)
+    for t in ring_tp + other_tp + (partner,):
         pl.semaphore_signal(barrier, inc=1, device_id=(ep, t), device_id_type=MESH)
 
     def weight_slots(core, who):
@@ -205,6 +208,9 @@
     ]
     if c == 0:
         own_mix = pltpu.make_async_copy(mix_in, xm.at[y, :, pl.ds(0, L)], misc.at[0])
+        own_mix.start()
+    else:
+        own_mix = pltpu.make_async_copy(mix_in, ymo, misc.at[0])
         own_mix.start()
     for copy in own_weights:
         copy.start()
@@ -246,12 +252,25 @@
     dsend[...] = outgoing.reshape(dsend.shape)
     ss[...] = jnp.zeros_like(ss)
 
-    pl.semaphore_wait(barrier, 2 * (n_ep - 1) + 3)
-
+    pl.semaphore_wait(barrier, 2 * (n_ep - 1) + 5)
+
+    own_mix.wait()
+    block = xm.at[y, :, pl.ds(0, L)] if c == 0 else ymo
+    first_tp = ring_tp if c == 0 else other_tp
+    mix_rows = rows_m // MIX_PARTS
+    for part in range(MIX_PARTS):
+        span = pl.ds(part * mix_rows, mix_rows)
+        for way in range(2):
+            if n_y > 2 or way == part % 2:
+                remote(
+                    block.at[span],
+                    xm.at[y, span, pl.ds(c * L, L)],
+                    misc.at[1 + way],
+                    ag_sem.at[part * long],
+                    (ep, first_tp[way]),
+                ).start()
     if c == 1:
-        give_mix = remote(
-            mix_in, xm.at[y, :, pl.ds(L, L)], misc.at[1], misc.at[2], (ep, partner)
-        )
+        give_mix = remote(ymo, xm.at[y, :, pl.ds(L, L)], s_sem.at[6], misc.at[7], (ep, partner))
         give_mix.start()
 
     def dispatch_copy(index, e):
@@ -278,7 +297,7 @@
 
     def gather_send(way, part, step):
         block = gather_block(way, part, step)
-        sem = ag_sem.at[place[way, part, step]]
+        sem = ag_sem.at[part * long + step]
         remote(block, block, s_sem.at[1], sem, (ep, ring_tp[way])).start()
 
     def gather_start(part):
@@ -287,9 +306,10 @@
                 gather_send(way, part, 0)
 
     def gather_step(step, some):
-        for way, part in order:
-            if part in some and step < hops(way, part):
-                received(gather_block(way, part, step + 1), ag_sem.at[place[way, part, step]])
+        for part in some:
+            ways = [way for way in range(2) if step < hops(way, part)]
+            received(x.at[0, pl.ds(0, len(ways) * rows)], ag_sem.at[part * long + step])
+            for way in ways:
                 if step + 1 < hops(way, part):
                     gather_send(way, part, step + 1)
 
@@ -318,10 +338,12 @@
     def sum_slot(way, part, step):
         return place[way, part, step - (long - hops(way, part))]
 
+    def sum_wait(part, step):
+        count = sum(step >= long - hops(way, part) for way in range(2))
+        received(recv.at[pl.ds(0, count)], rs_sem.at[part * long + step])
+
     def sum_in(way, part, step):
-        slot = sum_slot(way, part, step)
-        received(recv.at[slot], rs_sem.at[slot])
-        return recv[slot].astype(F32)
+        return recv[sum_slot(way, part, step)].astype(F32)
 
     def prepare(step, lo=0, hi=x.shape[1]):
         for way in range(2 if 0 < step < long else 1):
@@ -332,7 +354,11 @@
     def sum_sends(step, some):
         for way, part in last_first:
             first = long - hops(way, part)
-            if step < first or part not in some:
+            if part not in some:
+                continue
+            if way == 0 and step > 0:
+                sum_wait(part, step - 1)
+            if step < first:
                 continue
             value = pre[way if step > 0 else 0, part * rows : part * rows + rows]
             if step > first:
@@ -340,7 +366,11 @@
             slot = sum_slot(way, part, step)
             send[slot] = value.astype(BF16)
             remote(
-                send.at[slot], recv.at[slot], s_sem.at[2], rs_sem.at[slot], (ep, ring_tp[way])
+                send.at[slot],
+                recv.at[slot],
+                s_sem.at[2],
+                rs_sem.at[part * long + step],
+                (ep, ring_tp[way]),
             ).start()
 
     def sum_step(step):
@@ -349,6 +379,7 @@
 
     def sum_result(part):
         value = pre[0, part * rows : part * rows + rows]
+        sum_wait(part, long - 1)
         for way in range(2):
             if hops(way, part) > 0:
                 value = value + sum_in(way, part, long - 1)
@@ -361,10 +392,7 @@
         return (slot - row == group * (stride - cap)).astype(F32).astype(BF16)
 
     if c == 0:
-        own_mix.wait()
-        received(xm.at[y, :, pl.ds(L, L)], misc.at[2])
-        for part in range(parts):
-            gather_start(part)
+        received(ymo, misc.at[7])
         scale(y)
         for step in range(long):
             gather_step(step, range(parts))
@@ -437,11 +465,11 @@
             sum_step(step)
         if long == 1:
             pl.semaphore_wait(go.at[0], 1)
-        give_out = remote(ymo, ymo, misc.at[5], misc.at[6], (ep, partner))
+        give_out = remote(ysend, yrecv, misc.at[5], misc.at[6], (ep, partner))
         for part in range(parts):
             value = sum_result(part)
             out[part * rows : part * rows + rows, :] = value[:, :L]
-            ymo[part * rows : part * rows + rows, :] = value[:, L:]
+            ysend[part * rows : part * rows + rows, :] = value[:, L:]
         give_out.start()
     else:
 
@@ -470,10 +498,10 @@
 
         for part in range(parts):
             take_dispatch(part)
-            if part >= parts // 2 - 1:
-                gather_step(0, (part - parts // 2 + 1,))
+            if part >= parts // 2 + 1:
+                gather_step(0, (part - parts // 2 - 1,))
         scale(y)
-        gather_step(0, range(parts // 2 + 1, parts))
+        gather_step(0, range(parts // 2 - 1, parts))
         if long > 1:
             gather_step(1, range(parts))
         scale_step(0)
@@ -508,7 +536,7 @@
         spread_table = slot_table((n_x * stride, rows), 1)
         for part in reversed(range(parts)):
             spread = mm(spread_table, sum_result(part)).astype(BF16)
-            if part == 4:
+            if part == 7:
                 pl.semaphore_signal(
                     go.at[0], inc=1, device_id=(ep, partner), device_id_type=MESH
                 )
@@ -541,7 +569,9 @@
     for i in range(len(give_weights)):
         give_weights[i].wait_send()
     sent(dsend.at[pl.ds(0, n_ep - c)], s_sem.at[0])
-    sent(x.at[pl.ds(0, n_y - 1)], s_sem.at[1])
+    sent(ymo, misc.at[1])
+    sent(ymo, misc.at[2])
+    sent(x.at[pl.ds(0, n_y - (1, 3)[1 - c])], s_sem.at[1])
     sent(send, s_sem.at[2])
     if c == 0:
 
@@ -552,8 +582,8 @@
         give_out.wait_send()
     else:
         give_mix.wait_send()
-        received(ymo, misc.at[6])
-        out[pl.ds(0, rows_m), :] = ymo[...]
+        received(yrecv, misc.at[6])
+        out[pl.ds(0, rows_m), :] = yrecv[...]
         sent(rsend.at[0], s_sem.at[3])
         sent(rsend.at[1, pl.ds(0, n_ep - 1)], s_sem.at[4])
     received(dsend.at[pl.ds(0, n_ep - c)], s_sem.at[5])
@@ -628,19 +658,21 @@
         pltpu.VMEM((ex_slots, rows_e // Z, W), BF16),
         pltpu.VMEM((ex_slots, rows_e // Z, W), BF16),
         pltpu.VMEM((rows_m, L), BF16),
+        pltpu.VMEM((rows_m, L), BF16),
+        pltpu.VMEM((rows_m, L), BF16),
         pltpu.VMEM((2, n_ep, stride, L), BF16),
         pltpu.VMEM((n_ep, stride, L), BF16),
         pltpu.VMEM((2, rows_m, W), F32),
         pltpu.VMEM((2, rows_e, W), F32),
-        dma((ex_slots,)),
-        dma((ex_slots,)),
-        dma((6,)),
+        dma((Z * (n_y // 2),)),
+        dma((Z * (n_y // 2),)),
+        dma((7,)),
         dma((Z,)),
         dma((5,)),
         dma((5,)),
         dma((5,)),
         dma((4,)),
-        dma((7,)),
+        dma((8,)),
         pltpu.SemaphoreType.REGULAR((1,)),
         pltpu.VMEM((rows_m, 3 * W), F32),
     ]

time: 68.6 us -> 67.5 us (0.984)
  Pallas kernels: 66.5 us -> 65.4 us
    pallas_call x1, Pallas kernels: 66.5 us -> 65.4 us  [local(): pl.pallas_call(functools.partial(kernel, n_ep, n_y, cap, stride), out_sha...]
where the time goes in v4:
time: 67.5 us; the launch traced here: 67.3 us
  Pallas kernels  65.4 us (97%)
  local copies, waits for them, and re-layouts  1.27 us (2%)
    pallas_call x1, Pallas kernels, local(): pl.pallas_call(functools.partial(kernel, n_ep, n_y, cap, stride), out_sha...  65.4 us

profile of v4, /device:TPU:1, one launch (start us, length us, event | category | flops | bytes accessed | tf_op | source)
XLA Modules:
  0.0 67.3 jit_solution(9577441597440195111)
XLA Ops:
  0.6 65.4 %shard_map.149 = bf16[544,128]{1,0:T(8,128)(2,1)S(1)} custom-call(bf16[384,128]{1,0:T(8,128)(2,1)} %args_0_.4, f32[1,2048]{1,0:T(1,128)} %bitcast.14, bf16[2048,128]{1,0:T(8,128)(2,1)} %args_2_.4, bf16[2048,128]{1,0:T(8,128)(2,1)} %args_3_.4, bf16[2048,128]{1,0:T(8,128)(2,1)} %args_4_.4, f32[3,128]{1,0:T(4,128)} %args_5_.4, bf16[128,2048]{1,0:T(8,128)(2,1)} %args_6_.4, ...), custom_call_target="tpu_custom_call" | custom-call | tf_op jit(solution)/shard_map/pallas_call | solution.py:679
  66.1 0.6 slice.7
  66.7 0.6 slice.6

commit v5 on v4

--- a/solution.py
+++ b/solution.py
@@ -593,6 +593,18 @@
         term = mm(picks[k], back) * tcol[0:tok, 2 + k : 3 + k]
         total = term if total is None else total + term
     out[pl.ds(rows_m, tok), :] = total.astype(BF16)
+
+
+def deliver(both, mix_out, ex_out, sems):
+    rows = mix_out.shape[0]
+    copies = (
+        pltpu.make_async_copy(both.at[pl.ds(0, rows)], mix_out, sems.at[0]),
+        pltpu.make_async_copy(both.at[pl.ds(rows, ex_out.shape[0])], ex_out, sems.at[1]),
+    )
+    for copy in copies:
+        copy.start()
+    for copy in copies:
+        copy.wait()
 
 
 def local(
@@ -701,7 +713,16 @@
         jnp.swapaxes(expert_up, 1, 2)[0],
         expert_down[0],
     )
-    return both[: mix_input.shape[0]], both[mix_input.shape[0] :]
+    return pl.pallas_call(
+        deliver,
+        out_shape=(
+            jax.ShapeDtypeStruct(mix_input.shape, BF16),
+            jax.ShapeDtypeStruct(expert_input.shape, BF16),
+        ),
+        in_specs=[vmem],
+        out_specs=(any_spec, any_spec),
+        scratch_shapes=[dma((2,))],
+    )(pltpu.with_memory_space_constraint(both, pltpu.VMEM))
 
 
 def solution(mesh):

time: 67.5 us -> 67.1 us (level)
  local copies, waits for them, and re-layouts: 1.27 us -> 0 us
  Pallas kernels: 65.4 us -> 66.1 us
    slice x2 -> x0, local copies, waits for them, and re-layouts: 1.27 us -> none  [local(): return (both[:mix_input.shape[0]], both[mix_input.shape[0]:])]
where the time goes in v5:
time: 67.1 us; the launch traced here: 66.9 us
  Pallas kernels  66.1 us (99%)
  between operations  0.8 us (1%)
    pallas_call x1, Pallas kernels, local(): pl.pallas_call(functools.partial(kernel, n_ep, n_y, cap, stride), out_sha...  65.4 us

profile of v5, /device:TPU:1, one launch (start us, length us, event | category | flops | bytes accessed | tf_op | source)
XLA Modules:
  0.0 66.9 jit_solution(5939945318453627765)
XLA Ops:
  0.6 65.4 %shard_map.149.both = bf16[544,128]{1,0:T(8,128)(2,1)S(1)} custom-call(bf16[384,128]{1,0:T(8,128)(2,1)} %args_0_.4, f32[1,2048]{1,0:T(1,128)} %bitcast.14, bf16[2048,128]{1,0:T(8,128)(2,1)} %args_2_.4, bf16[2048,128]{1,0:T(8,128)(2,1)} %args_3_.4, bf16[2048,128]{1,0:T(8,128)(2,1)} %args_4_.4, f32[3,128]{1,0:T(4,128)} %args_5_.4, bf16[128,2048]{1,0:T(8,128)(2,1)} %args_6_.4, ...), custom_call_target="tpu_custom_call" | custom-call | tf_op jit(solution)/shard_map/pallas_call | solution.py:691
  66.1 0.7 %shard_map.150 = (bf16[384,128]{1,0:T(8,128)(2,1)}, bf16[160,128]{1,0:T(8,128)(2,1)}) custom-call(bf16[544,128]{1,0:T(8,128)(2,1)S(1)} %shard_map.149.both), custom_call_target="tpu_custom_call" | custom-call | tf_op jit(solution)/shard_map/pallas_call | solution.py:716
